TPU v7x, 512 devices: a 4x2x32 block of a 4x8x32 slice. The times are simulated.
512 devices in a mesh: grp: 2 (over y), sp: 64 (over z, core), tp: 4 (over x).
Axes of the slice: x: 4, y: 2, z: 32, core: 2. Of those that a mesh axis runs over, the one named last changes fastest.
The devices are a block of a 4x8x32 slice.
Arguments:
- query_latent: bfloat16 [16384, 768], P(('grp', 'sp')), parts along dimension 0, may hold values from -6 to 6
- key_latent: bfloat16 [16384, 256], P(('grp', 'sp', 'tp')), parts along dimension 0, may hold values from -20 to 20
- rotary_key: bfloat16 [16384, 64], P(('grp', 'sp', 'tp')), parts along dimension 0, may hold values from -1000 to 1000
- query_gain: float32 [768], replicated, may hold values from 0.1 to 1.9
- latent_gain: float32 [256], replicated, may hold values from 0.1 to 1.9
- query_up: bfloat16 [768, 3072], P(None, 'tp'), may hold values from -0.21875 to 0.21875
- key_up: bfloat16 [256, 2048], P(None, 'tp'), may hold values from -0.375 to 0.375
- value_up: bfloat16 [256, 2048], P(None, 'tp'), may hold values from -0.375 to 0.375
- out_gain: float32 [2048], P('tp'), may hold values from 0.1 to 1.9
- out_weight: bfloat16 [2048, 4096], P('sp', 'tp'), may hold values from -0.125 to 0.125
Outputs:
- mixed: bfloat16 [16384, 4096], P(('grp', 'sp'), 'tp'), parts along dimension 0
There are 2 independent parts, one for each index of `grp`. A program takes and returns all parts, laid end to end along the dimension named above; an argument that names none is the same for every part. Nothing has to cross between parts.
All inputs are finite; a program needn't handle non-finite values.
Results may differ from a plain program's by a relative error of at most 0.02.
The roundings to bfloat16 on the way count: a program that leaves them out, or rounds other values in their place, can miss the bound.
Values may be sent and summed in bfloat16 or wider, within the bound.
No kernel may reach another device: no remote copies, remote signals or barrier semaphores. Data moves between devices by JAX's collectives and lax.ppermute only.
A program may use at most 128 MiB of HBM per device.

v0:
```python
import functools

import jax
import jax.numpy as jnp
from jax import lax
from jax.experimental import pallas as pl
from jax.experimental.pallas import tpu as pltpu
from jax.sharding import Mesh
from jax.sharding import PartitionSpec as P


HEADS = 16
NOPE_DIM = 128
ROPE_DIM = 64
VALUE_DIM = 128
KVRANK = 256
CORES = 2


norm_eps = 1e-06
rope_theta = 10000.0
score_scale = (NOPE_DIM + ROPE_DIM) ** (-0.5)
exp2_scale = score_scale * 1.4426950408889634


def rms_scaled(inputs, gain_vec):
    widened = inputs.astype(jnp.float32)
    return (
        widened
        * lax.rsqrt(jnp.mean(widened * widened, axis=-1, keepdims=True) + norm_eps)
        * gain_vec
    )


def rotate_half(inputs, positions):
    half_width = inputs.shape[-1] // 2
    inverse = rope_theta ** (-jnp.arange(half_width, dtype=jnp.float32) / half_width)
    angles = positions[:, None] * inverse[None, :]
    if inputs.ndim == 3:
        angles = angles[:, None, :]
    cosine = jnp.cos(angles)
    sine = jnp.sin(angles)
    widened = inputs.astype(jnp.float32)
    first = widened[..., :half_width]
    second = widened[..., half_width:]
    return jnp.concatenate(
        [first * cosine - second * sine, second * cosine + first * sine], axis=-1
    )


def split_three(value):
    high = value.astype(jnp.bfloat16).astype(jnp.float32)
    rest = value - high
    middle = rest.astype(jnp.bfloat16).astype(jnp.float32)
    return high, middle, rest - middle


def as_row(column):
    return jnp.broadcast_to(column, (column.shape[0], 128)).T[:1, :]


def as_column(row):
    return jnp.broadcast_to(row, (128, row.shape[1])).T[:, :1]


def attend_kernel(guests, first, last, row_tile, *refs):
    query_refs, key_ref, refs = refs[:guests], refs[guests], refs[guests + 1 :]
    state_refs, outs = ((), refs) if first else (refs[: 2 * guests], refs[2 * guests :])
    rows = query_refs[0].shape[0]
    for guest in range(guests):
        blocks = []
        for begin in range(0, rows, row_tile):
            span = pl.ds(begin, row_tile)
            keys = key_ref[...]
            scores = lax.dot_general(
                query_refs[guest][span, :],
                keys,
                (((1,), (1,)), ((), ())),
                preferred_element_type=jnp.float32,
            )
            top = jnp.max(scores, axis=1, keepdims=True)
            if not first:
                stat_in, mix_in = state_refs[2 * guest : 2 * guest + 2]
                old_top = stat_in[span, :1]
                top = jnp.maximum(old_top, top)
            expo = jnp.exp2((scores - top) * exp2_scale)
            total = jnp.sum(expo, axis=1, keepdims=True)
            mix = jnp.dot(
                expo.astype(jnp.bfloat16),
                keys[:, :KVRANK],
                preferred_element_type=jnp.float32,
            )
            if not first:
                rescale = jnp.exp2((old_top - top) * exp2_scale)
                total = stat_in[span, 64:65] * rescale + total
                mix = mix_in[span, :] * rescale + mix
            if last:
                outs[0][span, :] = (mix / total).astype(jnp.bfloat16)
                place = lax.broadcasted_iota(jnp.int32, (8, row_tile), 0)
                block = jnp.zeros((8, row_tile), jnp.float32)
                for k, row in enumerate((*split_three(as_row(top)), *split_three(as_row(total)))):
                    block = jnp.where(place == k, row, block)
                blocks.append(block)
            else:
                lane = lax.broadcasted_iota(jnp.int32, (row_tile, 128), 1)
                outs[2 * guest][span, :] = jnp.where(lane < 64, top, total)
                outs[2 * guest + 1][span, :] = mix
        if last:
            outs[0][pl.ds(rows, 8 * len(blocks)), :] = jnp.concatenate(blocks, axis=0).astype(
                jnp.bfloat16
            )


def attend(queries, keys, state=(), last=False, row_tile=256):
    guests = len(queries)
    rows, width = queries[0].shape
    count = keys.shape[0]
    if last:
        shapes = (
            jax.ShapeDtypeStruct((rows + 8 * (rows // row_tile), KVRANK), jnp.bfloat16),
        )
    else:
        shapes = (
            jax.ShapeDtypeStruct((rows, 128), jnp.float32),
            jax.ShapeDtypeStruct((rows, KVRANK), jnp.float32),
        ) * guests
    return pl.pallas_call(
        functools.partial(attend_kernel, guests, not state, last, row_tile),
        out_shape=shapes,
        in_specs=[pl.BlockSpec(memory_space=pltpu.VMEM)] * (guests + 1 + len(state)),
        out_specs=tuple(pl.BlockSpec(memory_space=pltpu.VMEM) for _ in shapes),
        cost_estimate=pl.CostEstimate(
            flops=2 * guests * rows * count * (width + KVRANK),
            bytes_accessed=count * width * 2 + guests * rows * (width * 2 + KVRANK * 8),
            transcendentals=guests * rows * count,
        ),
        compiler_params=pltpu.CompilerParams(vmem_limit_bytes=20 * 1024 * 1024),
        name="attend",
    )(*queries, keys, *state)


def combine_kernel(row_tile, tokens, stat_ref, mix_ref, *refs):
    *part_refs, value_ref, gain_ref, out_ref = refs
    rows = mix_ref.shape[0]
    squares = jnp.zeros((tokens, 1), jnp.float32)
    for index, begin in enumerate(range(0, rows, row_tile)):
        span = pl.ds(begin, row_tile)
        tops = [stat_ref[span, :1]]
        sums = [stat_ref[span, 64:65]]
        for part_ref in part_refs:
            stats = part_ref[pl.ds(rows, 16), :].astype(jnp.float32)
            base = 8 * index
            top = stats[base : base + 1] + stats[base + 1 : base + 2] + stats[base + 2 : base + 3]
            total = (
                stats[base + 3 : base + 4] + stats[base + 4 : base + 5] + stats[base + 5 : base + 6]
            )
            tops.append(as_column(top))
            sums.append(as_column(total))
        best = functools.reduce(jnp.maximum, tops)
        rescale = jnp.exp2((tops[0] - best) * exp2_scale)
        whole = sums[0] * rescale
        mix = mix_ref[span, :] * rescale
        for part_ref, top, total in zip(part_refs, tops[1:], sums[1:]):
            weight = jnp.exp2((top - best) * exp2_scale) * total
            whole = whole + weight
            mix = mix + part_ref[span, :].astype(jnp.float32) * weight
        latent_mix = (mix / whole).astype(jnp.bfloat16)
        for offset in range(0, row_tile, tokens):
            head = (begin + offset) // tokens
            columns = pl.ds(head * VALUE_DIM, VALUE_DIM)
            head_out = jnp.dot(
                latent_mix[offset : offset + tokens],
                value_ref[:, columns],
                preferred_element_type=jnp.float32,
            ).astype(jnp.bfloat16)
            widened = head_out.astype(jnp.float32)
            squares = squares + jnp.sum(widened * widened, axis=1, keepdims=True)
            out_ref[:, columns] = (widened * gain_ref[:, columns]).astype(jnp.bfloat16)
    width = value_ref.shape[1]
    out_ref[:, pl.ds(width, 128)] = jnp.broadcast_to(squares, (tokens, 128)).astype(jnp.bfloat16)


def combine(state, parts, value_up, out_gain, tokens, row_tile=256):
    rows = state[1].shape[0]
    width = value_up.shape[1]
    return pl.pallas_call(
        functools.partial(combine_kernel, row_tile, tokens),
        out_shape=jax.ShapeDtypeStruct((tokens, width + 128), jnp.bfloat16),
        in_specs=[pl.BlockSpec(memory_space=pltpu.VMEM)] * (4 + len(parts)),
        out_specs=pl.BlockSpec(memory_space=pltpu.VMEM),
        cost_estimate=pl.CostEstimate(
            flops=2 * rows * KVRANK * VALUE_DIM,
            bytes_accessed=rows * KVRANK * 12,
            transcendentals=rows * 4,
        ),
        compiler_params=pltpu.CompilerParams(vmem_limit_bytes=16 * 1024 * 1024),
        name="combine",
    )(*state, *parts, value_up, out_gain[None, :])


def assemble_kernel(plan, n_in, *refs):
    sources, outs = refs[:n_in], refs[n_in:]
    for out, pieces in zip(outs, plan):
        at = 0
        for index, begin, count in pieces:
            out[pl.ds(at, count), :] = sources[index][pl.ds(begin, count), :]
            at += count


def assemble(sources, plan):
    shapes = tuple(
        jax.ShapeDtypeStruct((sum(p[2] for p in pieces), sources[0].shape[1]), sources[0].dtype)
        for pieces in plan
    )
    return pl.pallas_call(
        functools.partial(assemble_kernel, plan, len(sources)),
        out_shape=shapes,
        in_specs=[pl.BlockSpec(memory_space=pltpu.VMEM)] * len(sources),
        out_specs=tuple(pl.BlockSpec(memory_space=pltpu.VMEM) for _ in shapes),
        compiler_params=pltpu.CompilerParams(vmem_limit_bytes=8 * 1024 * 1024),
        name="assemble",
    )(*sources)


def prepare_kernel(
    latent_hbm, rotary_hbm, gain_hbm, cosine_ref, sine_ref, out_ref, latent_ref, rotary_ref, gain_ref, sems
):
    copies = [
        pltpu.make_async_copy(source, target, sems.at[k])
        for k, (source, target) in enumerate(
            ((latent_hbm, latent_ref), (rotary_hbm, rotary_ref), (gain_hbm, gain_ref))
        )
    ]
    for copy in copies:
        copy.start()
    for copy in copies:
        copy.wait()
    normed = rms_scaled(latent_ref[...], gain_ref[...])
    out_ref[:, :KVRANK] = normed.astype(jnp.bfloat16)
    widened = rotary_ref[...].astype(jnp.float32)
    half_width = ROPE_DIM // 2
    first, second = widened[:, :half_width], widened[:, half_width:]
    cosine, sine = cosine_ref[...], sine_ref[...]
    turned = jnp.concatenate(
        [first * cosine - second * sine, second * cosine + first * sine], axis=1
    )
    out_ref[:, KVRANK:] = turned.astype(jnp.bfloat16)


def prepare(key_latent, rotary_key, latent_gain, positions):
    rows = key_latent.shape[0]
    half_width = ROPE_DIM // 2
    inverse = rope_theta ** (-jnp.arange(half_width, dtype=jnp.float32) / half_width)
    angles = positions[:, None] * inverse[None, :]
    return pl.pallas_call(
        prepare_kernel,
        out_shape=jax.ShapeDtypeStruct((rows, KVRANK + ROPE_DIM), jnp.bfloat16),
        in_specs=[pl.BlockSpec(memory_space=pltpu.HBM)] * 3
        + [pl.BlockSpec(memory_space=pltpu.VMEM)] * 2,
        scratch_shapes=[
            pltpu.VMEM(key_latent.shape, key_latent.dtype),
            pltpu.VMEM(rotary_key.shape, rotary_key.dtype),
            pltpu.VMEM((1, latent_gain.shape[0]), latent_gain.dtype),
            pltpu.SemaphoreType.DMA((3,)),
        ],
        out_specs=pl.BlockSpec(memory_space=pltpu.VMEM),
        compiler_params=pltpu.CompilerParams(vmem_limit_bytes=8 * 1024 * 1024),
        name="prepare",
    )(key_latent, rotary_key, latent_gain[None, :], jnp.cos(angles), jnp.sin(angles))


def shifted(length, by):
    return [(i, (i + by) % length) for i in range(length)]


def on_device(
    chips,
    sides,
    query_latent,
    key_latent,
    rotary_key,
    query_gain,
    latent_gain,
    query_up,
    key_up,
    value_up,
    out_gain,
    out_weight,
):
    block_rows = query_latent.shape[0]
    row_count = key_latent.shape[0]
    head_local = key_up.shape[1] // NOPE_DIM
    block_start = (lax.axis_index("z") * CORES + lax.axis_index("core")) * block_rows
    own_start = block_start + lax.axis_index("tp") * row_count

    all_weight = lax.all_gather(out_weight, ("z", "core"), axis=0, tiled=True)

    own_positions = (own_start + jnp.arange(row_count, dtype=jnp.int32)).astype(jnp.float32)
    own = prepare(key_latent, rotary_key, latent_gain, own_positions)
    far = chips // 2
    others = []
    for by in (far, far // 2, -(far // 2)):
        others.append(lax.ppermute(own, "z", shifted(chips, by)))

    normed = rms_scaled(query_latent, query_gain).astype(jnp.bfloat16)
    query_full = jnp.dot(normed, query_up, preferred_element_type=jnp.float32)
    query_full = query_full.astype(jnp.bfloat16)
    query_full = query_full.reshape(block_rows, head_local, NOPE_DIM + ROPE_DIM)
    query_positions = (block_start + jnp.arange(block_rows, dtype=jnp.int32)).astype(jnp.float32)
    query_plain = query_full[..., :NOPE_DIM]
    query_turned = rotate_half(query_full[..., NOPE_DIM:], query_positions).astype(jnp.bfloat16)
    absorbed = jnp.einsum(
        "qhd,chd->hqc",
        query_plain,
        key_up.reshape(KVRANK, head_local, NOPE_DIM),
        preferred_element_type=jnp.float32,
    ).astype(jnp.bfloat16)
    queries = jnp.concatenate([absorbed, query_turned.transpose(1, 0, 2)], axis=-1)
    queries = queries.reshape(head_local * block_rows, KVRANK + ROPE_DIM)

    turns = (2, 1, -1)
    guests = []
    for by in turns:
        guests.append(lax.ppermute(queries, "tp", shifted(sides, by)))
    half = row_count // 2
    up, down = assemble(
        [own, *others], [[(k, begin, half) for k in range(4)] for begin in (0, half)]
    )
    distance = far // 4
    while distance > 1:
        up_next = lax.ppermute(up, "z", shifted(chips, distance))
        down_next = lax.ppermute(down, "z", shifted(chips, -distance))
        if distance == 2:
            up_next, down_next, *guests = lax.optimization_barrier((up_next, down_next, *guests))
        rows = up.shape[0]
        plan = [[(0, 0, rows), (1, 0, rows)], [(2, 0, rows), (3, 0, rows)]]
        if distance == 2:
            plan.append(plan[0] + plan[1])
        up, down, *near = assemble([up, up_next, down, down_next], plan)
        distance //= 2
    (near,) = near
    rows = up.shape[0]
    up_next = lax.ppermute(up, "z", shifted(chips, 1))
    down_next = lax.ppermute(down, "z", shifted(chips, -1))
    swap = [(i, (i + 1) % CORES) for i in range(CORES)]
    partner_near = lax.ppermute(near, "core", swap)
    everyone_asks = [*guests, queries]
    state = attend(everyone_asks, near)
    up_next, down_next, *state = lax.optimization_barrier((up_next, down_next, *state))
    (beside,) = assemble([up_next, down_next], [[(0, 0, rows), (1, 0, rows)]])
    partner_beside = lax.ppermute(beside, "core", swap)
    state = attend(everyone_asks, beside, state)
    state = attend(everyone_asks, partner_near, state)
    parts = []
    for k, by in enumerate(turns):
        (part,) = attend([guests[k]], partner_beside, state[2 * k : 2 * k + 2], last=True)
        parts.append(lax.ppermute(part, "tp", shifted(sides, -by)))
    state = attend([queries], partner_beside, state[2 * len(turns) :])
    sent = combine(state, parts, value_up, out_gain, block_rows)
    width = value_up.shape[1]
    everyone = lax.all_gather(sent, "tp", axis=0)
    all_squares = jnp.sum(everyone[:, :, width].astype(jnp.float32), axis=0)
    own_sums = jnp.einsum(
        "xtk,xkn->tn",
        everyone[:, :, :width],
        all_weight.reshape(sides, width, all_weight.shape[1]),
        preferred_element_type=jnp.float32,
    )
    mean_square = all_squares / (HEADS * VALUE_DIM)
    return (own_sums * lax.rsqrt(mean_square + norm_eps)[:, None]).astype(jnp.bfloat16)


def solution(mesh):
    groups, places, sides = (mesh.shape[name] for name in ("grp", "sp", "tp"))
    chips = places // CORES
    fine = Mesh(
        mesh.devices.reshape(groups, chips, CORES, sides), ("grp", "z", "core", "tp")
    )
    tokens = ("grp", "z", "core")
    in_specs = (
        P(tokens, None),
        P((*tokens, "tp"), None),
        P((*tokens, "tp"), None),
        P(),
        P(),
        P(None, "tp"),
        P(None, "tp"),
        P(None, "tp"),
        P("tp"),
        P(("z", "core"), "tp"),
    )
    return jax.shard_map(
        functools.partial(on_device, chips, sides),
        mesh=fine,
        in_specs=in_specs,
        out_specs=P(tokens, "tp"),
        check_vma=False,
    )
```

profile of v0, /device:TPU:33, one launch (start us, length us, event | category | flops | bytes accessed | tf_op | source)
XLA Modules:
  0.0 200.6 jit_solution(10001219151649803721)
XLA Ops:
  11.0 5.8 %collective-permute-start.7 = (bf16[512,320]{1,0:T(8,128)(2,1)S(1)}, bf16[512,320]{1,0:T(8,128)(2,1)S(1)}, u32[]{:S(2)}, u32[]{:S(2)}) collective-permute-start(bf16[512,320]{1,0:T(8,128)(2,1)S(1)} %bitcast.23), channel_id=1, source_target_pairs={{0,2},{1,3},{2,0},{3,1},{4,6},{5,7},{6,4},{7,5},{8,10},{9,11},{10,... | collective-permute-start | bytes 983048 | tf_op jit(solution)/shard_map/ppermute | solution.py:324
  16.8 2.4 %collective-permute-start.8 = (bf16[512,320]{1,0:T(8,128)(2,1)S(1)}, bf16[512,320]{1,0:T(8,128)(2,1)S(1)}, u32[]{:S(2)}, u32[]{:S(2)}) collective-permute-start(bf16[512,320]{1,0:T(8,128)(2,1)S(1)} %bitcast.24), channel_id=1, source_target_pairs={{0,1},{1,2},{2,3},{3,0},{4,5},{5,6},{6,7},{7,4},{8,9},{9,10},{10,1... | collective-permute-start | bytes 983048 | tf_op jit(solution)/shard_map/ppermute | solution.py:324
  19.2 4.2 %collective-permute-start.9 = (bf16[512,320]{1,0:T(8,128)(2,1)S(1)}, bf16[512,320]{1,0:T(8,128)(2,1)S(1)}, u32[]{:S(2)}, u32[]{:S(2)}) collective-permute-start(bf16[512,320]{1,0:T(8,128)(2,1)S(1)} %bitcast.25), channel_id=1, source_target_pairs={{0,3},{1,0},{2,1},{3,2},{4,7},{5,4},{6,5},{7,6},{8,11},{9,8},{10,9... | collective-permute-start | bytes 983048 | tf_op jit(solution)/shard_map/ppermute | solution.py:324
  23.8 42.5 %collective-permute-start = (bf16[32,320]{1,0:T(8,128)(2,1)S(1)}, bf16[32,320]{1,0:T(8,128)(2,1)S(1)}, u32[]{:S(2)}, u32[]{:S(2)}) collective-permute-start(bf16[32,320]{1,0:T(8,128)(2,1)S(1)} %prepare.1.refs_0_), channel_id=1, source_target_pairs={{0,128},{8,136},{16,144},{24,152},{32,160},{40,168},{48,176},{56,1... | collective-permute-start | bytes 61448 | tf_op jit(solution)/shard_map/ppermute | solution.py:303
  66.3 12.7 %collective-permute-start.1 = (bf16[32,320]{1,0:T(8,128)(2,1)S(1)}, bf16[32,320]{1,0:T(8,128)(2,1)S(1)}, u32[]{:S(2)}, u32[]{:S(2)}) collective-permute-start(bf16[32,320]{1,0:T(8,128)(2,1)S(1)} %prepare.1.refs_0_), channel_id=1, source_target_pairs={{0,64},{8,72},{16,80},{24,88},{32,96},{40,104},{48,112},{56,120},{... | collective-permute-start | bytes 61448 | tf_op jit(solution)/shard_map/ppermute | solution.py:303
  79.0 11.5 %collective-permute-start.2 = (bf16[32,320]{1,0:T(8,128)(2,1)S(1)}, bf16[32,320]{1,0:T(8,128)(2,1)S(1)}, u32[]{:S(2)}, u32[]{:S(2)}) collective-permute-start(bf16[32,320]{1,0:T(8,128)(2,1)S(1)} %prepare.1.refs_0_), channel_id=1, source_target_pairs={{0,192},{8,200},{16,208},{24,216},{32,224},{40,232},{48,240},{56,2... | collective-permute-start | bytes 61448 | tf_op jit(solution)/shard_map/ppermute | solution.py:303
  92.5 7.6 %collective-permute-start.3 = (bf16[64,320]{1,0:T(8,128)(2,1)S(1)}, bf16[64,320]{1,0:T(8,128)(2,1)S(1)}, u32[]{:S(2)}, u32[]{:S(2)}) collective-permute-start(bf16[64,320]{1,0:T(8,128)(2,1)S(1)} %get-tuple-element.53.refs_0_), channel_id=1, source_target_pairs={{0,32},{8,40},{16,48},{24,56},{32,64},{40,72},{48,80},{56,88},{64,... | collective-permute-start | bytes 122888 | tf_op jit(solution)/shard_map/ppermute | solution.py:331
  100.1 6.5 %collective-permute-start.4 = (bf16[64,320]{1,0:T(8,128)(2,1)S(1)}, bf16[64,320]{1,0:T(8,128)(2,1)S(1)}, u32[]{:S(2)}, u32[]{:S(2)}) collective-permute-start(bf16[64,320]{1,0:T(8,128)(2,1)S(1)} %get-tuple-element.54.refs_2_), channel_id=1, source_target_pairs={{0,224},{8,232},{16,240},{24,248},{32,0},{40,8},{48,16},{56,24},{6... | collective-permute-start | bytes 122888 | tf_op jit(solution)/shard_map/ppermute | solution.py:332
  106.6 2.5 %collective-permute-done.4.refs_3_ = bf16[64,320]{1,0:T(8,128)(2,1)S(1)} collective-permute-done((bf16[64,320]{1,0:T(8,128)(2,1)S(1)}, bf16[64,320]{1,0:T(8,128)(2,1)S(1)}, u32[]{:S(2)}, u32[]{:S(2)}) %collective-permute-start.4) | collective-permute-done | bytes 40992 | tf_op jit(solution)/shard_map/ppermute | solution.py:332
  109.1 4.7 %collective-permute-start.5 = (bf16[128,320]{1,0:T(8,128)(2,1)S(1)}, bf16[128,320]{1,0:T(8,128)(2,1)S(1)}, u32[]{:S(2)}, u32[]{:S(2)}) collective-permute-start(bf16[128,320]{1,0:T(8,128)(2,1)S(1)} %get-tuple-element.55.refs_0_), channel_id=1, source_target_pairs={{0,16},{8,24},{16,32},{24,40},{32,48},{40,56},{48,64},{56,72},{64,... | collective-permute-start | bytes 245768 | tf_op jit(solution)/shard_map/ppermute | solution.py:331
  113.8 4.9 %collective-permute-start.6 = (bf16[128,320]{1,0:T(8,128)(2,1)S(1)}, bf16[128,320]{1,0:T(8,128)(2,1)S(1)}, u32[]{:S(2)}, u32[]{:S(2)}) collective-permute-start(bf16[128,320]{1,0:T(8,128)(2,1)S(1)} %get-tuple-element.56.refs_2_), channel_id=1, source_target_pairs={{0,240},{8,248},{16,0},{24,8},{32,16},{40,24},{48,32},{56,40},{64,... | collective-permute-start | bytes 245768 | tf_op jit(solution)/shard_map/ppermute | solution.py:332
  118.9 2.0 %collective-permute-done.6.refs_3_ = bf16[128,320]{1,0:T(8,128)(2,1)S(1)} collective-permute-done((bf16[128,320]{1,0:T(8,128)(2,1)S(1)}, bf16[128,320]{1,0:T(8,128)(2,1)S(1)}, u32[]{:S(2)}, u32[]{:S(2)}) %collective-permute-start.6) | collective-permute-done | bytes 81952 | tf_op jit(solution)/shard_map/ppermute | solution.py:332
  121.0 3.7 %collective-permute-start.10 = (bf16[256,320]{1,0:T(8,128)(2,1)S(1)}, bf16[256,320]{1,0:T(8,128)(2,1)S(1)}, u32[]{:S(2)}, u32[]{:S(2)}) collective-permute-start(bf16[256,320]{1,0:T(8,128)(2,1)S(1)} %get-tuple-element.59), channel_id=1, source_target_pairs={{0,8},{8,16},{16,24},{24,32},{32,40},{40,48},{48,56},{56,64},{64,7... | collective-permute-start | bytes 491528 | tf_op jit(solution)/shard_map/ppermute | solution.py:343
  124.7 4.1 %collective-permute-start.11 = (bf16[256,320]{1,0:T(8,128)(2,1)S(1)}, bf16[256,320]{1,0:T(8,128)(2,1)S(1)}, u32[]{:S(2)}, u32[]{:S(2)}) collective-permute-start(bf16[256,320]{1,0:T(8,128)(2,1)S(1)} %get-tuple-element.60), channel_id=1, source_target_pairs={{0,248},{8,0},{16,8},{24,16},{32,24},{40,32},{48,40},{56,48},{64,5... | collective-permute-start | bytes 491528 | tf_op jit(solution)/shard_map/ppermute | solution.py:344
  128.8 12.2 %collective-permute-start.13 = (bf16[512,320]{1,0:T(8,128)(2,1)S(1)}, bf16[512,320]{1,0:T(8,128)(2,1)S(1)}, u32[]{:S(2)}, u32[]{:S(2)}) collective-permute-start(bf16[512,320]{1,0:T(8,128)(2,1)S(1)} %get-tuple-element.64.refs_4_), channel_id=1, source_target_pairs={{0,4},{4,0},{1,5},{5,1},{2,6},{6,2},{3,7},{7,3},{8,12},{12,8},{9,1... | collective-permute-start | bytes 983048 | tf_op jit(solution)/shard_map/ppermute | solution.py:346
  141.0 3.7 %attend.7 = (f32[512,128]{1,0:T(8,128)S(1)}, f32[512,256]{1,0:T(8,128)S(1)}, f32[512,128]{1,0:T(8,128)S(1)}, f32[512,256]{1,0:T(8,128)S(1)}, f32[512,128]{1,0:T(...) custom-call(bf16[512,320]{1,0:T(8,128)(2,1)S(1)} %collective-permute-done.7.refs_0_, ...), custom_call_target="tpu_custom_call" | custom-call | flops 1207959552 | bytes 5832704 | tf_op jit(solution)/shard_map/attend/pallas_call | solution.py:127
  144.8 2.1 %collective-permute-start.12 = (bf16[512,320]{1,0:T(8,128)(2,1)S(1)}, bf16[512,320]{1,0:T(8,128)(2,1)S(1)}, u32[]{:S(2)}, u32[]{:S(2)}) collective-permute-start(bf16[512,320]{1,0:T(8,128)(2,1)S(1)} %assemble.7.refs_4_), channel_id=1, source_target_pairs={{0,4},{4,0},{1,5},{5,1},{2,6},{6,2},{3,7},{7,3},{8,12},{12,8},{9,1... | collective-permute-start | bytes 983048 | tf_op jit(solution)/shard_map/ppermute | solution.py:351
  146.9 4.7 %attend.8 = (f32[512,128]{1,0:T(8,128)S(1)}, f32[512,256]{1,0:T(8,128)S(1)}, f32[512,128]{1,0:T(8,128)S(1)}, f32[512,256]{1,0:T(8,128)S(1)}, f32[512,128]{1,0:T(...) custom-call(bf16[512,320]{1,0:T(8,128)(2,1)S(1)} %collective-permute-done.7.refs_0_, ...), custom_call_target="tpu_custom_call" | custom-call | flops 1207959552 | bytes 5832704 | tf_op jit(solution)/shard_map/attend/pallas_call | solution.py:127
  151.7 4.7 %attend.9 = (f32[512,128]{1,0:T(8,128)S(1)}, f32[512,256]{1,0:T(8,128)S(1)}, f32[512,128]{1,0:T(8,128)S(1)}, f32[512,256]{1,0:T(8,128)S(1)}, f32[512,128]{1,0:T(...) custom-call(bf16[512,320]{1,0:T(8,128)(2,1)S(1)} %collective-permute-done.7.refs_0_, ...), custom_call_target="tpu_custom_call" | custom-call | flops 1207959552 | bytes 5832704 | tf_op jit(solution)/shard_map/attend/pallas_call | solution.py:127
  161.1 4.6 %collective-permute-start.15 = (bf16[528,256]{1,0:T(8,128)(2,1)S(1)}, bf16[528,256]{1,0:T(8,128)(2,1)S(1)}, u32[]{:S(2)}, u32[]{:S(2)}) collective-permute-start(bf16[528,256]{1,0:T(8,128)(2,1)S(1)} %attend.12), channel_id=1, source_target_pairs={{0,3},{1,0},{2,1},{3,2},{4,7},{5,4},{6,5},{7,6},{8,11},{9,8},{10,9... | collective-permute-start | bytes 811016 | tf_op jit(solution)/shard_map/ppermute | solution.py:357
  167.1 2.2 %collective-permute-start.14 = (bf16[528,256]{1,0:T(8,128)(2,1)S(1)}, bf16[528,256]{1,0:T(8,128)(2,1)S(1)}, u32[]{:S(2)}, u32[]{:S(2)}) collective-permute-start(bf16[528,256]{1,0:T(8,128)(2,1)S(1)} %attend.11), channel_id=1, source_target_pairs={{0,2},{1,3},{2,0},{3,1},{4,6},{5,7},{6,4},{7,5},{8,10},{9,11},{10,... | collective-permute-start | bytes 811016 | tf_op jit(solution)/shard_map/ppermute | solution.py:357
  171.2 6.3 %collective-permute-done.14.refs_0_ = bf16[528,256]{1,0:T(8,128)(2,1)S(1)} collective-permute-done((bf16[528,256]{1,0:T(8,128)(2,1)S(1)}, bf16[528,256]{1,0:T(8,128)(2,1)S(1)}, u32[]{:S(2)}, u32[]{:S(2)}) %collective-permute-start.14) | collective-permute-done | bytes 270368 | tf_op jit(solution)/shard_map/ppermute | solution.py:357
  179.3 10.7 %all-gather = bf16[512,640]{1,0:T(8,128)(2,1)S(1)} all-gather(bf16[128,640]{1,0:T(8,128)(2,1)S(1)} %combine.1), channel_id=2, replica_groups=mesh['grp'=2,'z'=32,'core'=2,'tp'=4] {'tp'}, dimensions={0}, use_global_device_ids=true | all-gather | bytes 819200 | tf_op jit(solution)/shard_map/all_gather | solution.py:361
  190.2 3.6 %fusion.1 = bf16[128,1024]{1,0:T(8,128)(2,1)} fusion(bf16[4,512,1024]{2,1,0:T(8,128)(2,1)} %bitcast.32, bf16[4,128,640]{2,1,0:T(8,128)(2,1)S(1)} %bitcast.34, f32[128]{0:T(128)S(1)} %add_rsqrt_fusion), kind=kOutput, calls=%fused_computation.3 | convolution fusion | flops 537133056 | bytes 4981248 | tf_op jit(solution)/shard_map/xtk,xkn->tn/dot_general | solution.py:363
  (60 shorter events, 16.9 us)
Async XLA Ops:
  6.6 4.1 %copy-start.6 = (bf16[256,512]{1,0:T(8,128)(2,1)S(1)}, bf16[256,512]{1,0:T(8,128)(2,1)}, u32[]{:S(2)}) copy-start(bf16[256,512]{1,0:T(8,128)(2,1)} %param.16) | copy-start | bytes 786436
  6.6 17.0 %copy-start.5 = (f32[256]{0:T(256)S(1)}, f32[256]{0:T(256)}, u32[]{:S(2)}) copy-start(f32[256]{0:T(256)} %param.14) | copy-start | bytes 3076
  6.6 17.0 %copy-start.2 = (bf16[32,256]{1,0:T(8,128)(2,1)S(1)}, bf16[32,256]{1,0:T(8,128)(2,1)}, u32[]{:S(2)}) copy-start(bf16[32,256]{1,0:T(8,128)(2,1)} %latent_hbm.1) | copy-start | bytes 49156
  6.6 17.0 %copy-start.3 = (bf16[32,64]{1,0:T(8,128)(2,1)S(1)}, bf16[32,64]{1,0:T(8,128)(2,1)}, u32[]{:S(2)}) copy-start(bf16[32,64]{1,0:T(8,128)(2,1)} %rotary_hbm.1) | copy-start | bytes 12292
  6.6 183.6 %all-gather.3.cloned.1.call-start = ((), (), s32[]{:S(2)}) async-start(), calls=%async_computation | async-start | bytes 4259840 | tf_op jit(solution)/shard_map/all_gather | solution.py:296
  11.0 109.9 %collective-permute-start.7 = (bf16[512,320]{1,0:T(8,128)(2,1)S(1)}, bf16[512,320]{1,0:T(8,128)(2,1)S(1)}, u32[]{:S(2)}, u32[]{:S(2)}) collective-permute-start(bf16[512,320]{1,0:T(8,128)(2,1)S(1)} %bitcast.23), channel_id=1, source_target_pairs={{0,2},{1,3},{2,0},{3,1},{4,6},{5,7},{6,4},{7,5},{8,10},{9,11},{10,... | collective-permute-start | bytes 983048 | tf_op jit(solution)/shard_map/ppermute | solution.py:324
  16.8 104.1 %collective-permute-start.8 = (bf16[512,320]{1,0:T(8,128)(2,1)S(1)}, bf16[512,320]{1,0:T(8,128)(2,1)S(1)}, u32[]{:S(2)}, u32[]{:S(2)}) collective-permute-start(bf16[512,320]{1,0:T(8,128)(2,1)S(1)} %bitcast.24), channel_id=1, source_target_pairs={{0,1},{1,2},{2,3},{3,0},{4,5},{5,6},{6,7},{7,4},{8,9},{9,10},{10,1... | collective-permute-start | bytes 983048 | tf_op jit(solution)/shard_map/ppermute | solution.py:324
  19.2 101.7 %collective-permute-start.9 = (bf16[512,320]{1,0:T(8,128)(2,1)S(1)}, bf16[512,320]{1,0:T(8,128)(2,1)S(1)}, u32[]{:S(2)}, u32[]{:S(2)}) collective-permute-start(bf16[512,320]{1,0:T(8,128)(2,1)S(1)} %bitcast.25), channel_id=1, source_target_pairs={{0,3},{1,0},{2,1},{3,2},{4,7},{5,4},{6,5},{7,6},{8,11},{9,8},{10,9... | collective-permute-start | bytes 983048 | tf_op jit(solution)/shard_map/ppermute | solution.py:324
  23.8 55.2 %collective-permute-start = (bf16[32,320]{1,0:T(8,128)(2,1)S(1)}, bf16[32,320]{1,0:T(8,128)(2,1)S(1)}, u32[]{:S(2)}, u32[]{:S(2)}) collective-permute-start(bf16[32,320]{1,0:T(8,128)(2,1)S(1)} %prepare.1.refs_0_), channel_id=1, source_target_pairs={{0,128},{8,136},{16,144},{24,152},{32,160},{40,168},{48,176},{56,1... | collective-permute-start | bytes 61448 | tf_op jit(solution)/shard_map/ppermute | solution.py:303
  66.3 24.2 %collective-permute-start.1 = (bf16[32,320]{1,0:T(8,128)(2,1)S(1)}, bf16[32,320]{1,0:T(8,128)(2,1)S(1)}, u32[]{:S(2)}, u32[]{:S(2)}) collective-permute-start(bf16[32,320]{1,0:T(8,128)(2,1)S(1)} %prepare.1.refs_0_), channel_id=1, source_target_pairs={{0,64},{8,72},{16,80},{24,88},{32,96},{40,104},{48,112},{56,120},{... | collective-permute-start | bytes 61448 | tf_op jit(solution)/shard_map/ppermute | solution.py:303
  79.0 13.4 %collective-permute-start.2 = (bf16[32,320]{1,0:T(8,128)(2,1)S(1)}, bf16[32,320]{1,0:T(8,128)(2,1)S(1)}, u32[]{:S(2)}, u32[]{:S(2)}) collective-permute-start(bf16[32,320]{1,0:T(8,128)(2,1)S(1)} %prepare.1.refs_0_), channel_id=1, source_target_pairs={{0,192},{8,200},{16,208},{24,216},{32,224},{40,232},{48,240},{56,2... | collective-permute-start | bytes 61448 | tf_op jit(solution)/shard_map/ppermute | solution.py:303
  92.5 14.1 %collective-permute-start.3 = (bf16[64,320]{1,0:T(8,128)(2,1)S(1)}, bf16[64,320]{1,0:T(8,128)(2,1)S(1)}, u32[]{:S(2)}, u32[]{:S(2)}) collective-permute-start(bf16[64,320]{1,0:T(8,128)(2,1)S(1)} %get-tuple-element.53.refs_0_), channel_id=1, source_target_pairs={{0,32},{8,40},{16,48},{24,56},{32,64},{40,72},{48,80},{56,88},{64,... | collective-permute-start | bytes 122888 | tf_op jit(solution)/shard_map/ppermute | solution.py:331
  100.1 9.0 %collective-permute-start.4 = (bf16[64,320]{1,0:T(8,128)(2,1)S(1)}, bf16[64,320]{1,0:T(8,128)(2,1)S(1)}, u32[]{:S(2)}, u32[]{:S(2)}) collective-permute-start(bf16[64,320]{1,0:T(8,128)(2,1)S(1)} %get-tuple-element.54.refs_2_), channel_id=1, source_target_pairs={{0,224},{8,232},{16,240},{24,248},{32,0},{40,8},{48,16},{56,24},{6... | collective-permute-start | bytes 122888 | tf_op jit(solution)/shard_map/ppermute | solution.py:332
  109.1 9.8 %collective-permute-start.5 = (bf16[128,320]{1,0:T(8,128)(2,1)S(1)}, bf16[128,320]{1,0:T(8,128)(2,1)S(1)}, u32[]{:S(2)}, u32[]{:S(2)}) collective-permute-start(bf16[128,320]{1,0:T(8,128)(2,1)S(1)} %get-tuple-element.55.refs_0_), channel_id=1, source_target_pairs={{0,16},{8,24},{16,32},{24,40},{32,48},{40,56},{48,64},{56,72},{64,... | collective-permute-start | bytes 245768 | tf_op jit(solution)/shard_map/ppermute | solution.py:331
  113.8 7.1 %collective-permute-start.6 = (bf16[128,320]{1,0:T(8,128)(2,1)S(1)}, bf16[128,320]{1,0:T(8,128)(2,1)S(1)}, u32[]{:S(2)}, u32[]{:S(2)}) collective-permute-start(bf16[128,320]{1,0:T(8,128)(2,1)S(1)} %get-tuple-element.56.refs_2_), channel_id=1, source_target_pairs={{0,240},{8,248},{16,0},{24,8},{32,16},{40,24},{48,32},{56,40},{64,... | collective-permute-start | bytes 245768 | tf_op jit(solution)/shard_map/ppermute | solution.py:332
  121.0 23.7 %collective-permute-start.10 = (bf16[256,320]{1,0:T(8,128)(2,1)S(1)}, bf16[256,320]{1,0:T(8,128)(2,1)S(1)}, u32[]{:S(2)}, u32[]{:S(2)}) collective-permute-start(bf16[256,320]{1,0:T(8,128)(2,1)S(1)} %get-tuple-element.59), channel_id=1, source_target_pairs={{0,8},{8,16},{16,24},{24,32},{32,40},{40,48},{48,56},{56,64},{64,7... | collective-permute-start | bytes 491528 | tf_op jit(solution)/shard_map/ppermute | solution.py:343
  124.7 20.1 %collective-permute-start.11 = (bf16[256,320]{1,0:T(8,128)(2,1)S(1)}, bf16[256,320]{1,0:T(8,128)(2,1)S(1)}, u32[]{:S(2)}, u32[]{:S(2)}) collective-permute-start(bf16[256,320]{1,0:T(8,128)(2,1)S(1)} %get-tuple-element.60), channel_id=1, source_target_pairs={{0,248},{8,0},{16,8},{24,16},{32,24},{40,32},{48,40},{56,48},{64,5... | collective-permute-start | bytes 491528 | tf_op jit(solution)/shard_map/ppermute | solution.py:344
  128.8 22.9 %collective-permute-start.13 = (bf16[512,320]{1,0:T(8,128)(2,1)S(1)}, bf16[512,320]{1,0:T(8,128)(2,1)S(1)}, u32[]{:S(2)}, u32[]{:S(2)}) collective-permute-start(bf16[512,320]{1,0:T(8,128)(2,1)S(1)} %get-tuple-element.64.refs_4_), channel_id=1, source_target_pairs={{0,4},{4,0},{1,5},{5,1},{2,6},{6,2},{3,7},{7,3},{8,12},{12,8},{9,1... | collective-permute-start | bytes 983048 | tf_op jit(solution)/shard_map/ppermute | solution.py:346
  144.8 11.6 %collective-permute-start.12 = (bf16[512,320]{1,0:T(8,128)(2,1)S(1)}, bf16[512,320]{1,0:T(8,128)(2,1)S(1)}, u32[]{:S(2)}, u32[]{:S(2)}) collective-permute-start(bf16[512,320]{1,0:T(8,128)(2,1)S(1)} %assemble.7.refs_4_), channel_id=1, source_target_pairs={{0,4},{4,0},{1,5},{5,1},{2,6},{6,2},{3,7},{7,3},{8,12},{12,8},{9,1... | collective-permute-start | bytes 983048 | tf_op jit(solution)/shard_map/ppermute | solution.py:351
  156.4 21.1 %copy-start.1 = (bf16[256,512]{1,0:T(8,128)(2,1)S(1)}, bf16[256,512]{1,0:T(8,128)(2,1)}, u32[]{:S(2)}) copy-start(bf16[256,512]{1,0:T(8,128)(2,1)} %refs_3_.1) | copy-start | bytes 786436
  156.4 21.1 %copy-start.4 = (f32[512]{0:T(512)S(1)}, f32[512]{0:T(512)}, u32[]{:S(2)}) copy-start(f32[512]{0:T(512)} %param.18) | copy-start | bytes 6148
  157.8 12.8 %collective-permute-start.16 = (bf16[528,256]{1,0:T(8,128)(2,1)S(1)}, bf16[528,256]{1,0:T(8,128)(2,1)S(1)}, u32[]{:S(2)}, u32[]{:S(2)}) collective-permute-start(bf16[528,256]{1,0:T(8,128)(2,1)S(1)} %attend.13), channel_id=1, source_target_pairs={{0,1},{1,2},{2,3},{3,0},{4,5},{5,6},{6,7},{7,4},{8,9},{9,10},{10,1... | collective-permute-start | bytes 811016 | tf_op jit(solution)/shard_map/ppermute | solution.py:357
  161.1 10.1 %collective-permute-start.15 = (bf16[528,256]{1,0:T(8,128)(2,1)S(1)}, bf16[528,256]{1,0:T(8,128)(2,1)S(1)}, u32[]{:S(2)}, u32[]{:S(2)}) collective-permute-start(bf16[528,256]{1,0:T(8,128)(2,1)S(1)} %attend.12), channel_id=1, source_target_pairs={{0,3},{1,0},{2,1},{3,2},{4,7},{5,4},{6,5},{7,6},{8,11},{9,8},{10,9... | collective-permute-start | bytes 811016 | tf_op jit(solution)/shard_map/ppermute | solution.py:357
  167.1 10.4 %collective-permute-start.14 = (bf16[528,256]{1,0:T(8,128)(2,1)S(1)}, bf16[528,256]{1,0:T(8,128)(2,1)S(1)}, u32[]{:S(2)}, u32[]{:S(2)}) collective-permute-start(bf16[528,256]{1,0:T(8,128)(2,1)S(1)} %attend.11), channel_id=1, source_target_pairs={{0,2},{1,3},{2,0},{3,1},{4,6},{5,7},{6,4},{7,5},{8,10},{9,11},{10,... | collective-permute-start | bytes 811016 | tf_op jit(solution)/shard_map/ppermute | solution.py:357
  (1 other events, 1.9 us)
Sparse Core Ops, SparseCore 0:
  9.5 168.8 all-gather.2
where the time goes:
time: 204 us; the launch traced here: 201 us
  starting transfers between devices  134 us (66%)
  Pallas kernels  20.7 us (10%)
  waiting for transfers between devices  14.3 us (7%)
  between operations  13.9 us (7%)
  blocking collectives  10.7 us (5%)
  matrix products  5.18 us (3%)
    ppermute x3, starting transfers between devices, on_device(): others.append(lax.ppermute(own, 'z', shifted(chips, by)))  66.7 us
    pallas_call x7, Pallas kernels, attend(): pl.pallas_call(functools.partial(attend_kernel, guests, not state, last,...  18.6 us
    ppermute x2, starting transfers between devices, on_device(): up_next = lax.ppermute(up, 'z', shifted(chips, distance))  12.3 us
    ppermute x3, starting transfers between devices, on_device(): guests.append(lax.ppermute(queries, 'tp', shifted(sides, by)))  12.3 us
    ppermute x1, starting transfers between devices, on_device(): partner_near = lax.ppermute(near, 'core', swap)  12.2 us
    ppermute x2, starting transfers between devices, on_device(): down_next = lax.ppermute(down, 'z', shifted(chips, -distance))  11.4 us
    all_gather x1, blocking collectives, on_device(): everyone = lax.all_gather(sent, 'tp', axis=0)  10.7 us
    ppermute x3, starting transfers between devices, on_device(): parts.append(lax.ppermute(part, 'tp', shifted(sides, -by)))  8.7 us
  transfers between devices with their start and end apart: 18, of which 6 were waited for; matrix products, arithmetic and copies ran while one was open for 2% of the time, Pallas kernels for 10%

commit v1 on v0

--- a/solution.py
+++ b/solution.py
@@ -55,80 +55,82 @@
     return high, middle, rest - middle
 
 
-def as_row(column):
-    return jnp.broadcast_to(column, (column.shape[0], 128)).T[:1, :]
-
-
 def as_column(row):
     return jnp.broadcast_to(row, (128, row.shape[1])).T[:, :1]
 
 
-def attend_kernel(guests, first, last, row_tile, *refs):
+def attend_kernel(guests, first, last, chunk, *refs):
     query_refs, key_ref, refs = refs[:guests], refs[guests], refs[guests + 1 :]
     state_refs, outs = ((), refs) if first else (refs[: 2 * guests], refs[2 * guests :])
     rows = query_refs[0].shape[0]
     for guest in range(guests):
+        stat_ref, mix_ref = outs[-2:] if last else outs[2 * guest : 2 * guest + 2]
+        keys = key_ref[...]
+        scores = lax.dot_general(
+            query_refs[guest][...],
+            keys,
+            (((1,), (1,)), ((), ())),
+            preferred_element_type=jnp.float32,
+        )
+        top = jnp.max(scores, axis=1, keepdims=True)
+        expo = jnp.exp2((scores - top) * exp2_scale)
+        total = jnp.sum(expo, axis=1, keepdims=True)
+        mix_ref[...] = jnp.dot(
+            expo.astype(jnp.bfloat16), keys[:, :KVRANK], preferred_element_type=jnp.float32
+        )
+        lane = lax.broadcasted_iota(jnp.int32, (rows, 128), 1)
+        stat_ref[...] = jnp.where(lane < 64, top, total)
+        if first:
+            continue
+        stat_in, mix_in = state_refs[2 * guest : 2 * guest + 2]
+        for begin in range(0, rows, chunk):
+            span = pl.ds(begin, chunk)
+            new, old = stat_ref[span, :], stat_in[span, :]
+            best = jnp.maximum(new[:, :1], old[:, :1])
+            new_scale = jnp.exp2((new[:, :1] - best) * exp2_scale)
+            old_scale = jnp.exp2((old[:, :1] - best) * exp2_scale)
+            mix = mix_ref[span, :] * new_scale + mix_in[span, :] * old_scale
+            totals = new * new_scale + old * old_scale
+            lane = lax.broadcasted_iota(jnp.int32, (chunk, 128), 1)
+            stat_ref[span, :] = jnp.where(lane < 64, best, totals)
+            if last:
+                outs[0][span, :] = (mix / totals[:, 64:65]).astype(jnp.bfloat16)
+            else:
+                mix_ref[span, :] = mix
+    if last:
+        width = mix_ref.shape[1]
         blocks = []
-        for begin in range(0, rows, row_tile):
-            span = pl.ds(begin, row_tile)
-            keys = key_ref[...]
-            scores = lax.dot_general(
-                query_refs[guest][span, :],
-                keys,
-                (((1,), (1,)), ((), ())),
-                preferred_element_type=jnp.float32,
-            )
-            top = jnp.max(scores, axis=1, keepdims=True)
-            if not first:
-                stat_in, mix_in = state_refs[2 * guest : 2 * guest + 2]
-                old_top = stat_in[span, :1]
-                top = jnp.maximum(old_top, top)
-            expo = jnp.exp2((scores - top) * exp2_scale)
-            total = jnp.sum(expo, axis=1, keepdims=True)
-            mix = jnp.dot(
-                expo.astype(jnp.bfloat16),
-                keys[:, :KVRANK],
-                preferred_element_type=jnp.float32,
-            )
-            if not first:
-                rescale = jnp.exp2((old_top - top) * exp2_scale)
-                total = stat_in[span, 64:65] * rescale + total
-                mix = mix_in[span, :] * rescale + mix
-            if last:
-                outs[0][span, :] = (mix / total).astype(jnp.bfloat16)
-                place = lax.broadcasted_iota(jnp.int32, (8, row_tile), 0)
-                block = jnp.zeros((8, row_tile), jnp.float32)
-                for k, row in enumerate((*split_three(as_row(top)), *split_three(as_row(total)))):
-                    block = jnp.where(place == k, row, block)
-                blocks.append(block)
-            else:
-                lane = lax.broadcasted_iota(jnp.int32, (row_tile, 128), 1)
-                outs[2 * guest][span, :] = jnp.where(lane < 64, top, total)
-                outs[2 * guest + 1][span, :] = mix
-        if last:
-            outs[0][pl.ds(rows, 8 * len(blocks)), :] = jnp.concatenate(blocks, axis=0).astype(
-                jnp.bfloat16
-            )
-
-
-def attend(queries, keys, state=(), last=False, row_tile=256):
+        for begin in range(0, rows, width):
+            turned = stat_ref[pl.ds(begin, width), :].T
+            place = lax.broadcasted_iota(jnp.int32, (8, width), 0)
+            block = jnp.zeros((8, width), jnp.float32)
+            for k, row in enumerate((*split_three(turned[:1]), *split_three(turned[64:65]))):
+                block = jnp.where(place == k, row, block)
+            blocks.append(block)
+        outs[0][pl.ds(rows, 8 * len(blocks)), :] = jnp.concatenate(blocks, axis=0).astype(
+            jnp.bfloat16
+        )
+
+
+def attend(queries, keys, state=(), last=False):
     guests = len(queries)
     rows, width = queries[0].shape
     count = keys.shape[0]
+    scratch = []
     if last:
-        shapes = (
-            jax.ShapeDtypeStruct((rows + 8 * (rows // row_tile), KVRANK), jnp.bfloat16),
-        )
+        shapes = (jax.ShapeDtypeStruct((rows + 8 * (rows // KVRANK), KVRANK), jnp.bfloat16),)
+        scratch = [pltpu.VMEM((rows, 128), jnp.float32), pltpu.VMEM((rows, KVRANK), jnp.float32)]
     else:
         shapes = (
             jax.ShapeDtypeStruct((rows, 128), jnp.float32),
             jax.ShapeDtypeStruct((rows, KVRANK), jnp.float32),
         ) * guests
     return pl.pallas_call(
-        functools.partial(attend_kernel, guests, not state, last, row_tile),
+        functools.partial(attend_kernel, guests, not state, last, 64),
         out_shape=shapes,
         in_specs=[pl.BlockSpec(memory_space=pltpu.VMEM)] * (guests + 1 + len(state)),
         out_specs=tuple(pl.BlockSpec(memory_space=pltpu.VMEM) for _ in shapes),
+        scratch_shapes=scratch,
         cost_estimate=pl.CostEstimate(
             flops=2 * guests * rows * count * (width + KVRANK),
             bytes_accessed=count * width * 2 + guests * rows * (width * 2 + KVRANK * 8),

time: 204 us -> 201 us (0.985)
  Pallas kernels: 20.7 us -> 17.6 us
    pallas_call x7, Pallas kernels: 18.6 us -> 15.5 us  [attend(): pl.pallas_call(functools.partial(attend_kernel, guests, not state, last,...]
  transfers between devices with their start and end apart: 18 -> 18, of which waited for: 6 -> 6; matrix products, arithmetic and copies ran while one was open for 2% -> 2% of each run, Pallas kernels for 10% -> 9%
where the time goes in v1:
time: 201 us; the launch traced here: 198 us
  starting transfers between devices  134 us (67%)
  Pallas kernels  17.6 us (9%)
  waiting for transfers between devices  14.3 us (7%)
  between operations  13.9 us (7%)
  blocking collectives  10.9 us (5%)
  matrix products  5.17 us (3%)
    ppermute x3, starting transfers between devices, on_device(): others.append(lax.ppermute(own, 'z', shifted(chips, by)))  66.7 us
    pallas_call x7, Pallas kernels, attend(): pl.pallas_call(functools.partial(attend_kernel, guests, not state, last,...  15.5 us
    ppermute x2, starting transfers between devices, on_device(): up_next = lax.ppermute(up, 'z', shifted(chips, distance))  12.3 us
    ppermute x3, starting transfers between devices, on_device(): guests.append(lax.ppermute(queries, 'tp', shifted(sides, by)))  12.3 us
    ppermute x1, starting transfers between devices, on_device(): partner_near = lax.ppermute(near, 'core', swap)  12.2 us
    ppermute x2, starting transfers between devices, on_device(): down_next = lax.ppermute(down, 'z', shifted(chips, -distance))  11.4 us
    all_gather x1, blocking collectives, on_device(): everyone = lax.all_gather(sent, 'tp', axis=0)  10.9 us
    ppermute x3, starting transfers between devices, on_device(): parts.append(lax.ppermute(part, 'tp', shifted(sides, -by)))  8.73 us
  transfers between devices with their start and end apart: 18, of which 6 were waited for; matrix products, arithmetic and copies ran while one was open for 2% of the time, Pallas kernels for 9%

profile of v1, /device:TPU:33, one launch (start us, length us, event | category | flops | bytes accessed | tf_op | source)
XLA Modules:
  0.0 197.7 jit_solution(4794663802307901276)
XLA Ops:
  11.0 5.8 %collective-permute-start.7 = (bf16[512,320]{1,0:T(8,128)(2,1)S(1)}, bf16[512,320]{1,0:T(8,128)(2,1)S(1)}, u32[]{:S(2)}, u32[]{:S(2)}) collective-permute-start(bf16[512,320]{1,0:T(8,128)(2,1)S(1)} %bitcast.23), channel_id=1, source_target_pairs={{0,2},{1,3},{2,0},{3,1},{4,6},{5,7},{6,4},{7,5},{8,10},{9,11},{10,... | collective-permute-start | bytes 983048 | tf_op jit(solution)/shard_map/ppermute | solution.py:326
  16.8 2.4 %collective-permute-start.8 = (bf16[512,320]{1,0:T(8,128)(2,1)S(1)}, bf16[512,320]{1,0:T(8,128)(2,1)S(1)}, u32[]{:S(2)}, u32[]{:S(2)}) collective-permute-start(bf16[512,320]{1,0:T(8,128)(2,1)S(1)} %bitcast.24), channel_id=1, source_target_pairs={{0,1},{1,2},{2,3},{3,0},{4,5},{5,6},{6,7},{7,4},{8,9},{9,10},{10,1... | collective-permute-start | bytes 983048 | tf_op jit(solution)/shard_map/ppermute | solution.py:326
  19.2 4.2 %collective-permute-start.9 = (bf16[512,320]{1,0:T(8,128)(2,1)S(1)}, bf16[512,320]{1,0:T(8,128)(2,1)S(1)}, u32[]{:S(2)}, u32[]{:S(2)}) collective-permute-start(bf16[512,320]{1,0:T(8,128)(2,1)S(1)} %bitcast.25), channel_id=1, source_target_pairs={{0,3},{1,0},{2,1},{3,2},{4,7},{5,4},{6,5},{7,6},{8,11},{9,8},{10,9... | collective-permute-start | bytes 983048 | tf_op jit(solution)/shard_map/ppermute | solution.py:326
  23.8 42.5 %collective-permute-start = (bf16[32,320]{1,0:T(8,128)(2,1)S(1)}, bf16[32,320]{1,0:T(8,128)(2,1)S(1)}, u32[]{:S(2)}, u32[]{:S(2)}) collective-permute-start(bf16[32,320]{1,0:T(8,128)(2,1)S(1)} %prepare.1.refs_0_), channel_id=1, source_target_pairs={{0,128},{8,136},{16,144},{24,152},{32,160},{40,168},{48,176},{56,1... | collective-permute-start | bytes 61448 | tf_op jit(solution)/shard_map/ppermute | solution.py:305
  66.3 12.7 %collective-permute-start.1 = (bf16[32,320]{1,0:T(8,128)(2,1)S(1)}, bf16[32,320]{1,0:T(8,128)(2,1)S(1)}, u32[]{:S(2)}, u32[]{:S(2)}) collective-permute-start(bf16[32,320]{1,0:T(8,128)(2,1)S(1)} %prepare.1.refs_0_), channel_id=1, source_target_pairs={{0,64},{8,72},{16,80},{24,88},{32,96},{40,104},{48,112},{56,120},{... | collective-permute-start | bytes 61448 | tf_op jit(solution)/shard_map/ppermute | solution.py:305
  79.0 11.5 %collective-permute-start.2 = (bf16[32,320]{1,0:T(8,128)(2,1)S(1)}, bf16[32,320]{1,0:T(8,128)(2,1)S(1)}, u32[]{:S(2)}, u32[]{:S(2)}) collective-permute-start(bf16[32,320]{1,0:T(8,128)(2,1)S(1)} %prepare.1.refs_0_), channel_id=1, source_target_pairs={{0,192},{8,200},{16,208},{24,216},{32,224},{40,232},{48,240},{56,2... | collective-permute-start | bytes 61448 | tf_op jit(solution)/shard_map/ppermute | solution.py:305
  92.5 7.6 %collective-permute-start.3 = (bf16[64,320]{1,0:T(8,128)(2,1)S(1)}, bf16[64,320]{1,0:T(8,128)(2,1)S(1)}, u32[]{:S(2)}, u32[]{:S(2)}) collective-permute-start(bf16[64,320]{1,0:T(8,128)(2,1)S(1)} %get-tuple-element.53.refs_0_), channel_id=1, source_target_pairs={{0,32},{8,40},{16,48},{24,56},{32,64},{40,72},{48,80},{56,88},{64,... | collective-permute-start | bytes 122888 | tf_op jit(solution)/shard_map/ppermute | solution.py:333
  100.1 6.5 %collective-permute-start.4 = (bf16[64,320]{1,0:T(8,128)(2,1)S(1)}, bf16[64,320]{1,0:T(8,128)(2,1)S(1)}, u32[]{:S(2)}, u32[]{:S(2)}) collective-permute-start(bf16[64,320]{1,0:T(8,128)(2,1)S(1)} %get-tuple-element.54.refs_2_), channel_id=1, source_target_pairs={{0,224},{8,232},{16,240},{24,248},{32,0},{40,8},{48,16},{56,24},{6... | collective-permute-start | bytes 122888 | tf_op jit(solution)/shard_map/ppermute | solution.py:334
  106.6 2.5 %collective-permute-done.4.refs_3_ = bf16[64,320]{1,0:T(8,128)(2,1)S(1)} collective-permute-done((bf16[64,320]{1,0:T(8,128)(2,1)S(1)}, bf16[64,320]{1,0:T(8,128)(2,1)S(1)}, u32[]{:S(2)}, u32[]{:S(2)}) %collective-permute-start.4) | collective-permute-done | bytes 40992 | tf_op jit(solution)/shard_map/ppermute | solution.py:334
  109.1 4.7 %collective-permute-start.5 = (bf16[128,320]{1,0:T(8,128)(2,1)S(1)}, bf16[128,320]{1,0:T(8,128)(2,1)S(1)}, u32[]{:S(2)}, u32[]{:S(2)}) collective-permute-start(bf16[128,320]{1,0:T(8,128)(2,1)S(1)} %get-tuple-element.55.refs_0_), channel_id=1, source_target_pairs={{0,16},{8,24},{16,32},{24,40},{32,48},{40,56},{48,64},{56,72},{64,... | collective-permute-start | bytes 245768 | tf_op jit(solution)/shard_map/ppermute | solution.py:333
  113.8 4.9 %collective-permute-start.6 = (bf16[128,320]{1,0:T(8,128)(2,1)S(1)}, bf16[128,320]{1,0:T(8,128)(2,1)S(1)}, u32[]{:S(2)}, u32[]{:S(2)}) collective-permute-start(bf16[128,320]{1,0:T(8,128)(2,1)S(1)} %get-tuple-element.56.refs_2_), channel_id=1, source_target_pairs={{0,240},{8,248},{16,0},{24,8},{32,16},{40,24},{48,32},{56,40},{64,... | collective-permute-start | bytes 245768 | tf_op jit(solution)/shard_map/ppermute | solution.py:334
  118.9 2.0 %collective-permute-done.6.refs_3_ = bf16[128,320]{1,0:T(8,128)(2,1)S(1)} collective-permute-done((bf16[128,320]{1,0:T(8,128)(2,1)S(1)}, bf16[128,320]{1,0:T(8,128)(2,1)S(1)}, u32[]{:S(2)}, u32[]{:S(2)}) %collective-permute-start.6) | collective-permute-done | bytes 81952 | tf_op jit(solution)/shard_map/ppermute | solution.py:334
  121.0 3.7 %collective-permute-start.10 = (bf16[256,320]{1,0:T(8,128)(2,1)S(1)}, bf16[256,320]{1,0:T(8,128)(2,1)S(1)}, u32[]{:S(2)}, u32[]{:S(2)}) collective-permute-start(bf16[256,320]{1,0:T(8,128)(2,1)S(1)} %get-tuple-element.59), channel_id=1, source_target_pairs={{0,8},{8,16},{16,24},{24,32},{32,40},{40,48},{48,56},{56,64},{64,7... | collective-permute-start | bytes 491528 | tf_op jit(solution)/shard_map/ppermute | solution.py:345
  124.7 4.1 %collective-permute-start.11 = (bf16[256,320]{1,0:T(8,128)(2,1)S(1)}, bf16[256,320]{1,0:T(8,128)(2,1)S(1)}, u32[]{:S(2)}, u32[]{:S(2)}) collective-permute-start(bf16[256,320]{1,0:T(8,128)(2,1)S(1)} %get-tuple-element.60), channel_id=1, source_target_pairs={{0,248},{8,0},{16,8},{24,16},{32,24},{40,32},{48,40},{56,48},{64,5... | collective-permute-start | bytes 491528 | tf_op jit(solution)/shard_map/ppermute | solution.py:346
  128.8 12.2 %collective-permute-start.13 = (bf16[512,320]{1,0:T(8,128)(2,1)S(1)}, bf16[512,320]{1,0:T(8,128)(2,1)S(1)}, u32[]{:S(2)}, u32[]{:S(2)}) collective-permute-start(bf16[512,320]{1,0:T(8,128)(2,1)S(1)} %get-tuple-element.64.refs_4_), channel_id=1, source_target_pairs={{0,4},{4,0},{1,5},{5,1},{2,6},{6,2},{3,7},{7,3},{8,12},{12,8},{9,1... | collective-permute-start | bytes 983048 | tf_op jit(solution)/shard_map/ppermute | solution.py:348
  141.0 2.7 %attend.7 = (f32[512,128]{1,0:T(8,128)S(1)}, f32[512,256]{1,0:T(8,128)S(1)}, f32[512,128]{1,0:T(8,128)S(1)}, f32[512,256]{1,0:T(8,128)S(1)}, f32[512,128]{1,0:T(...) custom-call(bf16[512,320]{1,0:T(8,128)(2,1)S(1)} %collective-permute-done.7.refs_0_, ...), custom_call_target="tpu_custom_call" | custom-call | flops 1207959552 | bytes 5832704 | tf_op jit(solution)/shard_map/attend/pallas_call | solution.py:128
  143.8 2.1 %collective-permute-start.12 = (bf16[512,320]{1,0:T(8,128)(2,1)S(1)}, bf16[512,320]{1,0:T(8,128)(2,1)S(1)}, u32[]{:S(2)}, u32[]{:S(2)}) collective-permute-start(bf16[512,320]{1,0:T(8,128)(2,1)S(1)} %assemble.7.refs_4_), channel_id=1, source_target_pairs={{0,4},{4,0},{1,5},{5,1},{2,6},{6,2},{3,7},{7,3},{8,12},{12,8},{9,1... | collective-permute-start | bytes 983048 | tf_op jit(solution)/shard_map/ppermute | solution.py:353
  145.9 3.4 %attend.8 = (f32[512,128]{1,0:T(8,128)S(1)}, f32[512,256]{1,0:T(8,128)S(1)}, f32[512,128]{1,0:T(8,128)S(1)}, f32[512,256]{1,0:T(8,128)S(1)}, f32[512,128]{1,0:T(...) custom-call(bf16[512,320]{1,0:T(8,128)(2,1)S(1)} %collective-permute-done.7.refs_0_, ...), custom_call_target="tpu_custom_call" | custom-call | flops 1207959552 | bytes 5832704 | tf_op jit(solution)/shard_map/attend/pallas_call | solution.py:128
  149.3 3.4 %attend.9 = (f32[512,128]{1,0:T(8,128)S(1)}, f32[512,256]{1,0:T(8,128)S(1)}, f32[512,128]{1,0:T(8,128)S(1)}, f32[512,256]{1,0:T(8,128)S(1)}, f32[512,128]{1,0:T(...) custom-call(bf16[512,320]{1,0:T(8,128)(2,1)S(1)} %collective-permute-done.7.refs_0_, ...), custom_call_target="tpu_custom_call" | custom-call | flops 1207959552 | bytes 5832704 | tf_op jit(solution)/shard_map/attend/pallas_call | solution.py:128
  157.9 4.6 %collective-permute-start.15 = (bf16[528,256]{1,0:T(8,128)(2,1)S(1)}, bf16[528,256]{1,0:T(8,128)(2,1)S(1)}, u32[]{:S(2)}, u32[]{:S(2)}) collective-permute-start(bf16[528,256]{1,0:T(8,128)(2,1)S(1)} %attend.12), channel_id=1, source_target_pairs={{0,3},{1,0},{2,1},{3,2},{4,7},{5,4},{6,5},{7,6},{8,11},{9,8},{10,9... | collective-permute-start | bytes 811016 | tf_op jit(solution)/shard_map/ppermute | solution.py:359
  164.0 2.2 %collective-permute-start.14 = (bf16[528,256]{1,0:T(8,128)(2,1)S(1)}, bf16[528,256]{1,0:T(8,128)(2,1)S(1)}, u32[]{:S(2)}, u32[]{:S(2)}) collective-permute-start(bf16[528,256]{1,0:T(8,128)(2,1)S(1)} %attend.11), channel_id=1, source_target_pairs={{0,2},{1,3},{2,0},{3,1},{4,6},{5,7},{6,4},{7,5},{8,10},{9,11},{10,... | collective-permute-start | bytes 811016 | tf_op jit(solution)/shard_map/ppermute | solution.py:359
  167.7 6.7 %collective-permute-done.14.refs_0_ = bf16[528,256]{1,0:T(8,128)(2,1)S(1)} collective-permute-done((bf16[528,256]{1,0:T(8,128)(2,1)S(1)}, bf16[528,256]{1,0:T(8,128)(2,1)S(1)}, u32[]{:S(2)}, u32[]{:S(2)}) %collective-permute-start.14) | collective-permute-done | bytes 270368 | tf_op jit(solution)/shard_map/ppermute | solution.py:359
  176.2 10.9 %all-gather = bf16[512,640]{1,0:T(8,128)(2,1)S(1)} all-gather(bf16[128,640]{1,0:T(8,128)(2,1)S(1)} %combine.1), channel_id=2, replica_groups=mesh['grp'=2,'z'=32,'core'=2,'tp'=4] {'tp'}, dimensions={0}, use_global_device_ids=true | all-gather | bytes 819200 | tf_op jit(solution)/shard_map/all_gather | solution.py:363
  187.2 3.6 %fusion.1 = bf16[128,1024]{1,0:T(8,128)(2,1)} fusion(bf16[4,512,1024]{2,1,0:T(8,128)(2,1)} %bitcast.32, bf16[4,128,640]{2,1,0:T(8,128)(2,1)S(1)} %bitcast.34, f32[128]{0:T(128)S(1)} %add_rsqrt_fusion), kind=kOutput, calls=%fused_computation.3 | convolution fusion | flops 537133056 | bytes 4981248 | tf_op jit(solution)/shard_map/xtk,xkn->tn/dot_general | solution.py:365
  (60 shorter events, 17.0 us)
Async XLA Ops:
  6.6 4.1 %copy-start.6 = (bf16[256,512]{1,0:T(8,128)(2,1)S(1)}, bf16[256,512]{1,0:T(8,128)(2,1)}, u32[]{:S(2)}) copy-start(bf16[256,512]{1,0:T(8,128)(2,1)} %param.16) | copy-start | bytes 786436
  6.6 17.0 %copy-start.5 = (f32[256]{0:T(256)S(1)}, f32[256]{0:T(256)}, u32[]{:S(2)}) copy-start(f32[256]{0:T(256)} %param.14) | copy-start | bytes 3076
  6.6 17.0 %copy-start.2 = (bf16[32,256]{1,0:T(8,128)(2,1)S(1)}, bf16[32,256]{1,0:T(8,128)(2,1)}, u32[]{:S(2)}) copy-start(bf16[32,256]{1,0:T(8,128)(2,1)} %latent_hbm.1) | copy-start | bytes 49156
  6.6 17.0 %copy-start.3 = (bf16[32,64]{1,0:T(8,128)(2,1)S(1)}, bf16[32,64]{1,0:T(8,128)(2,1)}, u32[]{:S(2)}) copy-start(bf16[32,64]{1,0:T(8,128)(2,1)} %rotary_hbm.1) | copy-start | bytes 12292
  6.6 180.7 %all-gather.3.cloned.1.call-start = ((), (), s32[]{:S(2)}) async-start(), calls=%async_computation | async-start | bytes 4259840 | tf_op jit(solution)/shard_map/all_gather | solution.py:298
  11.0 109.9 %collective-permute-start.7 = (bf16[512,320]{1,0:T(8,128)(2,1)S(1)}, bf16[512,320]{1,0:T(8,128)(2,1)S(1)}, u32[]{:S(2)}, u32[]{:S(2)}) collective-permute-start(bf16[512,320]{1,0:T(8,128)(2,1)S(1)} %bitcast.23), channel_id=1, source_target_pairs={{0,2},{1,3},{2,0},{3,1},{4,6},{5,7},{6,4},{7,5},{8,10},{9,11},{10,... | collective-permute-start | bytes 983048 | tf_op jit(solution)/shard_map/ppermute | solution.py:326
  16.8 104.1 %collective-permute-start.8 = (bf16[512,320]{1,0:T(8,128)(2,1)S(1)}, bf16[512,320]{1,0:T(8,128)(2,1)S(1)}, u32[]{:S(2)}, u32[]{:S(2)}) collective-permute-start(bf16[512,320]{1,0:T(8,128)(2,1)S(1)} %bitcast.24), channel_id=1, source_target_pairs={{0,1},{1,2},{2,3},{3,0},{4,5},{5,6},{6,7},{7,4},{8,9},{9,10},{10,1... | collective-permute-start | bytes 983048 | tf_op jit(solution)/shard_map/ppermute | solution.py:326
  19.2 101.7 %collective-permute-start.9 = (bf16[512,320]{1,0:T(8,128)(2,1)S(1)}, bf16[512,320]{1,0:T(8,128)(2,1)S(1)}, u32[]{:S(2)}, u32[]{:S(2)}) collective-permute-start(bf16[512,320]{1,0:T(8,128)(2,1)S(1)} %bitcast.25), channel_id=1, source_target_pairs={{0,3},{1,0},{2,1},{3,2},{4,7},{5,4},{6,5},{7,6},{8,11},{9,8},{10,9... | collective-permute-start | bytes 983048 | tf_op jit(solution)/shard_map/ppermute | solution.py:326
  23.8 55.2 %collective-permute-start = (bf16[32,320]{1,0:T(8,128)(2,1)S(1)}, bf16[32,320]{1,0:T(8,128)(2,1)S(1)}, u32[]{:S(2)}, u32[]{:S(2)}) collective-permute-start(bf16[32,320]{1,0:T(8,128)(2,1)S(1)} %prepare.1.refs_0_), channel_id=1, source_target_pairs={{0,128},{8,136},{16,144},{24,152},{32,160},{40,168},{48,176},{56,1... | collective-permute-start | bytes 61448 | tf_op jit(solution)/shard_map/ppermute | solution.py:305
  66.3 24.2 %collective-permute-start.1 = (bf16[32,320]{1,0:T(8,128)(2,1)S(1)}, bf16[32,320]{1,0:T(8,128)(2,1)S(1)}, u32[]{:S(2)}, u32[]{:S(2)}) collective-permute-start(bf16[32,320]{1,0:T(8,128)(2,1)S(1)} %prepare.1.refs_0_), channel_id=1, source_target_pairs={{0,64},{8,72},{16,80},{24,88},{32,96},{40,104},{48,112},{56,120},{... | collective-permute-start | bytes 61448 | tf_op jit(solution)/shard_map/ppermute | solution.py:305
  79.0 13.4 %collective-permute-start.2 = (bf16[32,320]{1,0:T(8,128)(2,1)S(1)}, bf16[32,320]{1,0:T(8,128)(2,1)S(1)}, u32[]{:S(2)}, u32[]{:S(2)}) collective-permute-start(bf16[32,320]{1,0:T(8,128)(2,1)S(1)} %prepare.1.refs_0_), channel_id=1, source_target_pairs={{0,192},{8,200},{16,208},{24,216},{32,224},{40,232},{48,240},{56,2... | collective-permute-start | bytes 61448 | tf_op jit(solution)/shard_map/ppermute | solution.py:305
  92.5 14.1 %collective-permute-start.3 = (bf16[64,320]{1,0:T(8,128)(2,1)S(1)}, bf16[64,320]{1,0:T(8,128)(2,1)S(1)}, u32[]{:S(2)}, u32[]{:S(2)}) collective-permute-start(bf16[64,320]{1,0:T(8,128)(2,1)S(1)} %get-tuple-element.53.refs_0_), channel_id=1, source_target_pairs={{0,32},{8,40},{16,48},{24,56},{32,64},{40,72},{48,80},{56,88},{64,... | collective-permute-start | bytes 122888 | tf_op jit(solution)/shard_map/ppermute | solution.py:333
  100.1 9.0 %collective-permute-start.4 = (bf16[64,320]{1,0:T(8,128)(2,1)S(1)}, bf16[64,320]{1,0:T(8,128)(2,1)S(1)}, u32[]{:S(2)}, u32[]{:S(2)}) collective-permute-start(bf16[64,320]{1,0:T(8,128)(2,1)S(1)} %get-tuple-element.54.refs_2_), channel_id=1, source_target_pairs={{0,224},{8,232},{16,240},{24,248},{32,0},{40,8},{48,16},{56,24},{6... | collective-permute-start | bytes 122888 | tf_op jit(solution)/shard_map/ppermute | solution.py:334
  109.1 9.8 %collective-permute-start.5 = (bf16[128,320]{1,0:T(8,128)(2,1)S(1)}, bf16[128,320]{1,0:T(8,128)(2,1)S(1)}, u32[]{:S(2)}, u32[]{:S(2)}) collective-permute-start(bf16[128,320]{1,0:T(8,128)(2,1)S(1)} %get-tuple-element.55.refs_0_), channel_id=1, source_target_pairs={{0,16},{8,24},{16,32},{24,40},{32,48},{40,56},{48,64},{56,72},{64,... | collective-permute-start | bytes 245768 | tf_op jit(solution)/shard_map/ppermute | solution.py:333
  113.8 7.1 %collective-permute-start.6 = (bf16[128,320]{1,0:T(8,128)(2,1)S(1)}, bf16[128,320]{1,0:T(8,128)(2,1)S(1)}, u32[]{:S(2)}, u32[]{:S(2)}) collective-permute-start(bf16[128,320]{1,0:T(8,128)(2,1)S(1)} %get-tuple-element.56.refs_2_), channel_id=1, source_target_pairs={{0,240},{8,248},{16,0},{24,8},{32,16},{40,24},{48,32},{56,40},{64,... | collective-permute-start | bytes 245768 | tf_op jit(solution)/shard_map/ppermute | solution.py:334
  121.0 22.7 %collective-permute-start.10 = (bf16[256,320]{1,0:T(8,128)(2,1)S(1)}, bf16[256,320]{1,0:T(8,128)(2,1)S(1)}, u32[]{:S(2)}, u32[]{:S(2)}) collective-permute-start(bf16[256,320]{1,0:T(8,128)(2,1)S(1)} %get-tuple-element.59), channel_id=1, source_target_pairs={{0,8},{8,16},{16,24},{24,32},{32,40},{40,48},{48,56},{56,64},{64,7... | collective-permute-start | bytes 491528 | tf_op jit(solution)/shard_map/ppermute | solution.py:345
  124.7 19.1 %collective-permute-start.11 = (bf16[256,320]{1,0:T(8,128)(2,1)S(1)}, bf16[256,320]{1,0:T(8,128)(2,1)S(1)}, u32[]{:S(2)}, u32[]{:S(2)}) collective-permute-start(bf16[256,320]{1,0:T(8,128)(2,1)S(1)} %get-tuple-element.60), channel_id=1, source_target_pairs={{0,248},{8,0},{16,8},{24,16},{32,24},{40,32},{48,40},{56,48},{64,5... | collective-permute-start | bytes 491528 | tf_op jit(solution)/shard_map/ppermute | solution.py:346
  128.8 20.5 %collective-permute-start.13 = (bf16[512,320]{1,0:T(8,128)(2,1)S(1)}, bf16[512,320]{1,0:T(8,128)(2,1)S(1)}, u32[]{:S(2)}, u32[]{:S(2)}) collective-permute-start(bf16[512,320]{1,0:T(8,128)(2,1)S(1)} %get-tuple-element.64.refs_4_), channel_id=1, source_target_pairs={{0,4},{4,0},{1,5},{5,1},{2,6},{6,2},{3,7},{7,3},{8,12},{12,8},{9,1... | collective-permute-start | bytes 983048 | tf_op jit(solution)/shard_map/ppermute | solution.py:348
  143.8 9.0 %collective-permute-start.12 = (bf16[512,320]{1,0:T(8,128)(2,1)S(1)}, bf16[512,320]{1,0:T(8,128)(2,1)S(1)}, u32[]{:S(2)}, u32[]{:S(2)}) collective-permute-start(bf16[512,320]{1,0:T(8,128)(2,1)S(1)} %assemble.7.refs_4_), channel_id=1, source_target_pairs={{0,4},{4,0},{1,5},{5,1},{2,6},{6,2},{3,7},{7,3},{8,12},{12,8},{9,1... | collective-permute-start | bytes 983048 | tf_op jit(solution)/shard_map/ppermute | solution.py:353
  152.8 21.6 %copy-start.1 = (bf16[256,512]{1,0:T(8,128)(2,1)S(1)}, bf16[256,512]{1,0:T(8,128)(2,1)}, u32[]{:S(2)}) copy-start(bf16[256,512]{1,0:T(8,128)(2,1)} %refs_3_.1) | copy-start | bytes 786436
  152.8 21.6 %copy-start.4 = (f32[512]{0:T(512)S(1)}, f32[512]{0:T(512)}, u32[]{:S(2)}) copy-start(f32[512]{0:T(512)} %param.18) | copy-start | bytes 6148
  154.4 13.2 %collective-permute-start.16 = (bf16[528,256]{1,0:T(8,128)(2,1)S(1)}, bf16[528,256]{1,0:T(8,128)(2,1)S(1)}, u32[]{:S(2)}, u32[]{:S(2)}) collective-permute-start(bf16[528,256]{1,0:T(8,128)(2,1)S(1)} %attend.13), channel_id=1, source_target_pairs={{0,1},{1,2},{2,3},{3,0},{4,5},{5,6},{6,7},{7,4},{8,9},{9,10},{10,1... | collective-permute-start | bytes 811016 | tf_op jit(solution)/shard_map/ppermute | solution.py:359
  157.9 9.9 %collective-permute-start.15 = (bf16[528,256]{1,0:T(8,128)(2,1)S(1)}, bf16[528,256]{1,0:T(8,128)(2,1)S(1)}, u32[]{:S(2)}, u32[]{:S(2)}) collective-permute-start(bf16[528,256]{1,0:T(8,128)(2,1)S(1)} %attend.12), channel_id=1, source_target_pairs={{0,3},{1,0},{2,1},{3,2},{4,7},{5,4},{6,5},{7,6},{8,11},{9,8},{10,9... | collective-permute-start | bytes 811016 | tf_op jit(solution)/shard_map/ppermute | solution.py:359
  164.0 10.4 %collective-permute-start.14 = (bf16[528,256]{1,0:T(8,128)(2,1)S(1)}, bf16[528,256]{1,0:T(8,128)(2,1)S(1)}, u32[]{:S(2)}, u32[]{:S(2)}) collective-permute-start(bf16[528,256]{1,0:T(8,128)(2,1)S(1)} %attend.11), channel_id=1, source_target_pairs={{0,2},{1,3},{2,0},{3,1},{4,6},{5,7},{6,4},{7,5},{8,10},{9,11},{10,... | collective-permute-start | bytes 811016 | tf_op jit(solution)/shard_map/ppermute | solution.py:359
  (1 other events, 1.9 us)
Sparse Core Ops, SparseCore 0:
  9.5 168.7 all-gather.2

commit v2 on v1

--- a/solution.py
+++ b/solution.py
@@ -271,6 +271,66 @@
     )(key_latent, rotary_key, latent_gain[None, :], jnp.cos(angles), jnp.sin(angles))
 
 
+def project_kernel(
+    blocks, everyone_hbm, weight_hbm, out_ref, everyone_ref, weight_ref, total, sems
+):
+    depth = weight_ref.shape[0] // blocks
+    sides, _, width = everyone_ref.shape
+    width -= 128
+    shared = width // depth
+    activations = pltpu.make_async_copy(everyone_hbm, everyone_ref, sems.at[blocks])
+    activations.start()
+    copies = []
+    for block in range(blocks):
+        span = pl.ds(block * depth, depth)
+        copies.append(
+            pltpu.make_async_copy(weight_hbm.at[span, :], weight_ref.at[span, :], sems.at[block])
+        )
+        copies[-1].start()
+    activations.wait()
+    squares = sum(
+        everyone_ref[side, :, pl.ds(width, 128)].astype(jnp.float32) for side in range(sides)
+    )
+    scale = lax.rsqrt(squares[:, :1] / (HEADS * VALUE_DIM) + norm_eps)
+    for block in range(blocks):
+        copies[block].wait()
+        product = jnp.dot(
+            everyone_ref[block // shared, :, pl.ds(block % shared * depth, depth)],
+            weight_ref[pl.ds(block * depth, depth), :],
+            preferred_element_type=jnp.float32,
+        )
+        if block == 0:
+            total[...] = product
+        elif block < blocks - 1:
+            total[...] += product
+        else:
+            out_ref[...] = ((total[...] + product) * scale).astype(jnp.bfloat16)
+
+
+def project(everyone, weight, blocks=8):
+    tokens = everyone.shape[1]
+    depth, features = weight.shape
+    return pl.pallas_call(
+        functools.partial(project_kernel, blocks),
+        out_shape=jax.ShapeDtypeStruct((tokens, features), jnp.bfloat16),
+        in_specs=[pl.BlockSpec(memory_space=pltpu.HBM)] * 2,
+        out_specs=pl.BlockSpec(memory_space=pltpu.VMEM),
+        scratch_shapes=[
+            pltpu.VMEM(everyone.shape, everyone.dtype),
+            pltpu.VMEM(weight.shape, weight.dtype),
+            pltpu.VMEM((tokens, features), jnp.float32),
+            pltpu.SemaphoreType.DMA((blocks + 1,)),
+        ],
+        cost_estimate=pl.CostEstimate(
+            flops=2 * tokens * depth * features,
+            bytes_accessed=depth * features * 2,
+            transcendentals=0,
+        ),
+        compiler_params=pltpu.CompilerParams(vmem_limit_bytes=60 * 1024 * 1024),
+        name="project",
+    )(everyone, weight)
+
+
 def shifted(length, by):
     return [(i, (i + by) % length) for i in range(length)]
 
@@ -332,8 +392,6 @@
     while distance > 1:
         up_next = lax.ppermute(up, "z", shifted(chips, distance))
         down_next = lax.ppermute(down, "z", shifted(chips, -distance))
-        if distance == 2:
-            up_next, down_next, *guests = lax.optimization_barrier((up_next, down_next, *guests))
         rows = up.shape[0]
         plan = [[(0, 0, rows), (1, 0, rows)], [(2, 0, rows), (3, 0, rows)]]
         if distance == 2:
@@ -359,17 +417,8 @@
         parts.append(lax.ppermute(part, "tp", shifted(sides, -by)))
     state = attend([queries], partner_beside, state[2 * len(turns) :])
     sent = combine(state, parts, value_up, out_gain, block_rows)
-    width = value_up.shape[1]
     everyone = lax.all_gather(sent, "tp", axis=0)
-    all_squares = jnp.sum(everyone[:, :, width].astype(jnp.float32), axis=0)
-    own_sums = jnp.einsum(
-        "xtk,xkn->tn",
-        everyone[:, :, :width],
-        all_weight.reshape(sides, width, all_weight.shape[1]),
-        preferred_element_type=jnp.float32,
-    )
-    mean_square = all_squares / (HEADS * VALUE_DIM)
-    return (own_sums * lax.rsqrt(mean_square + norm_eps)[:, None]).astype(jnp.bfloat16)
+    return project(everyone, all_weight)
 
 
 def solution(mesh):

time: 201 us -> 199 us (0.990)
  matrix products: 5.17 us -> 1.56 us
  Pallas kernels: 17.6 us -> 20.8 us
    dot_general x1 -> x0, matrix products: 3.61 us -> none  [on_device(): jnp.einsum('xtk,xkn->tn', everyone[:, :, :width], all_weight.reshape(side...]
    pallas_call x0 -> x1, Pallas kernels: none -> 3.36 us  [project(): pl.pallas_call(functools.partial(project_kernel, blocks), out_shape=jax.S...]
    ppermute x1, starting transfers between devices: 12.2 us -> 9.61 us  [on_device(): partner_near = lax.ppermute(near, 'core', swap)]
  transfers between devices with their start and end apart: 18 -> 18, of which waited for: 6 -> 5; matrix products, arithmetic and copies ran while one was open for 2% -> 2% of each run, Pallas kernels for 9% -> 9%
where the time goes in v2:
time: 199 us; the launch traced here: 196 us
  starting transfers between devices  132 us (66%)
  Pallas kernels  20.8 us (10%)
  between operations  13.9 us (7%)
  waiting for transfers between devices  13.5 us (7%)
  blocking collectives  12.2 us (6%)
    ppermute x3, starting transfers between devices, on_device(): others.append(lax.ppermute(own, 'z', shifted(chips, by)))  67.5 us
    pallas_call x7, Pallas kernels, attend(): pl.pallas_call(functools.partial(attend_kernel, guests, not state, last,...  15.4 us
    ppermute x2, starting transfers between devices, on_device(): down_next = lax.ppermute(down, 'z', shifted(chips, -distance))  13.1 us
    ppermute x2, starting transfers between devices, on_device(): up_next = lax.ppermute(up, 'z', shifted(chips, distance))  12.7 us
    all_gather x1, blocking collectives, on_device(): everyone = lax.all_gather(sent, 'tp', axis=0)  12.2 us
    ppermute x3, starting transfers between devices, on_device(): guests.append(lax.ppermute(queries, 'tp', shifted(sides, by)))  11.1 us
    ppermute x1, starting transfers between devices, on_device(): partner_near = lax.ppermute(near, 'core', swap)  9.61 us
    ppermute x3, starting transfers between devices, on_device(): parts.append(lax.ppermute(part, 'tp', shifted(sides, -by)))  8.86 us
  transfers between devices with their start and end apart: 18, of which 5 were waited for; matrix products, arithmetic and copies ran while one was open for 2% of the time, Pallas kernels for 9%

profile of v2, /device:TPU:33, one launch (start us, length us, event | category | flops | bytes accessed | tf_op | source)
XLA Modules:
  0.0 196.0 jit_solution(15895613914879899583)
XLA Ops:
  11.1 4.1 %collective-permute-start.10 = (bf16[512,320]{1,0:T(8,128)(2,1)S(1)}, bf16[512,320]{1,0:T(8,128)(2,1)S(1)}, u32[]{:S(2)}, u32[]{:S(2)}) collective-permute-start(bf16[512,320]{1,0:T(8,128)(2,1)S(1)} %bitcast.15), channel_id=1, source_target_pairs={{0,1},{1,2},{2,3},{3,0},{4,5},{5,6},{6,7},{7,4},{8,9},{9,10},{10,1... | collective-permute-start | bytes 983048 | tf_op jit(solution)/shard_map/ppermute | solution.py:386
  15.2 3.5 %collective-permute-start.11 = (bf16[512,320]{1,0:T(8,128)(2,1)S(1)}, bf16[512,320]{1,0:T(8,128)(2,1)S(1)}, u32[]{:S(2)}, u32[]{:S(2)}) collective-permute-start(bf16[512,320]{1,0:T(8,128)(2,1)S(1)} %bitcast.16), channel_id=1, source_target_pairs={{0,3},{1,0},{2,1},{3,2},{4,7},{5,4},{6,5},{7,6},{8,11},{9,8},{10,9... | collective-permute-start | bytes 983048 | tf_op jit(solution)/shard_map/ppermute | solution.py:386
  18.7 3.5 %collective-permute-start.9 = (bf16[512,320]{1,0:T(8,128)(2,1)S(1)}, bf16[512,320]{1,0:T(8,128)(2,1)S(1)}, u32[]{:S(2)}, u32[]{:S(2)}) collective-permute-start(bf16[512,320]{1,0:T(8,128)(2,1)S(1)} %bitcast.17), channel_id=1, source_target_pairs={{0,2},{1,3},{2,0},{3,1},{4,6},{5,7},{6,4},{7,5},{8,10},{9,11},{10,... | collective-permute-start | bytes 983048 | tf_op jit(solution)/shard_map/ppermute | solution.py:386
  22.7 42.5 %collective-permute-start = (bf16[32,320]{1,0:T(8,128)(2,1)S(1)}, bf16[32,320]{1,0:T(8,128)(2,1)S(1)}, u32[]{:S(2)}, u32[]{:S(2)}) collective-permute-start(bf16[32,320]{1,0:T(8,128)(2,1)S(1)} %prepare.1.refs_0_), channel_id=1, source_target_pairs={{0,128},{8,136},{16,144},{24,152},{32,160},{40,168},{48,176},{56,1... | collective-permute-start | bytes 61448 | tf_op jit(solution)/shard_map/ppermute | solution.py:365
  65.2 12.7 %collective-permute-start.1 = (bf16[32,320]{1,0:T(8,128)(2,1)S(1)}, bf16[32,320]{1,0:T(8,128)(2,1)S(1)}, u32[]{:S(2)}, u32[]{:S(2)}) collective-permute-start(bf16[32,320]{1,0:T(8,128)(2,1)S(1)} %prepare.1.refs_0_), channel_id=1, source_target_pairs={{0,64},{8,72},{16,80},{24,88},{32,96},{40,104},{48,112},{56,120},{... | collective-permute-start | bytes 61448 | tf_op jit(solution)/shard_map/ppermute | solution.py:365
  77.9 12.3 %collective-permute-start.2 = (bf16[32,320]{1,0:T(8,128)(2,1)S(1)}, bf16[32,320]{1,0:T(8,128)(2,1)S(1)}, u32[]{:S(2)}, u32[]{:S(2)}) collective-permute-start(bf16[32,320]{1,0:T(8,128)(2,1)S(1)} %prepare.1.refs_0_), channel_id=1, source_target_pairs={{0,192},{8,200},{16,208},{24,216},{32,224},{40,232},{48,240},{56,2... | collective-permute-start | bytes 61448 | tf_op jit(solution)/shard_map/ppermute | solution.py:365
  91.4 7.5 %collective-permute-start.3 = (bf16[64,320]{1,0:T(8,128)(2,1)S(1)}, bf16[64,320]{1,0:T(8,128)(2,1)S(1)}, u32[]{:S(2)}, u32[]{:S(2)}) collective-permute-start(bf16[64,320]{1,0:T(8,128)(2,1)S(1)} %get-tuple-element.48.refs_0_), channel_id=1, source_target_pairs={{0,32},{8,40},{16,48},{24,56},{32,64},{40,72},{48,80},{56,88},{64,... | collective-permute-start | bytes 122888 | tf_op jit(solution)/shard_map/ppermute | solution.py:393
  98.9 7.3 %collective-permute-start.4 = (bf16[64,320]{1,0:T(8,128)(2,1)S(1)}, bf16[64,320]{1,0:T(8,128)(2,1)S(1)}, u32[]{:S(2)}, u32[]{:S(2)}) collective-permute-start(bf16[64,320]{1,0:T(8,128)(2,1)S(1)} %get-tuple-element.49.refs_2_), channel_id=1, source_target_pairs={{0,224},{8,232},{16,240},{24,248},{32,0},{40,8},{48,16},{56,24},{6... | collective-permute-start | bytes 122888 | tf_op jit(solution)/shard_map/ppermute | solution.py:394
  107.8 5.2 %collective-permute-start.5 = (bf16[128,320]{1,0:T(8,128)(2,1)S(1)}, bf16[128,320]{1,0:T(8,128)(2,1)S(1)}, u32[]{:S(2)}, u32[]{:S(2)}) collective-permute-start(bf16[128,320]{1,0:T(8,128)(2,1)S(1)} %get-tuple-element.50.refs_0_), channel_id=1, source_target_pairs={{0,16},{8,24},{16,32},{24,40},{32,48},{40,56},{48,64},{56,72},{64,... | collective-permute-start | bytes 245768 | tf_op jit(solution)/shard_map/ppermute | solution.py:393
  113.0 5.8 %collective-permute-start.6 = (bf16[128,320]{1,0:T(8,128)(2,1)S(1)}, bf16[128,320]{1,0:T(8,128)(2,1)S(1)}, u32[]{:S(2)}, u32[]{:S(2)}) collective-permute-start(bf16[128,320]{1,0:T(8,128)(2,1)S(1)} %get-tuple-element.51.refs_2_), channel_id=1, source_target_pairs={{0,240},{8,248},{16,0},{24,8},{32,16},{40,24},{48,32},{56,40},{64,... | collective-permute-start | bytes 245768 | tf_op jit(solution)/shard_map/ppermute | solution.py:394
  119.6 2.4 %collective-permute-done.6.refs_3_ = bf16[128,320]{1,0:T(8,128)(2,1)S(1)} collective-permute-done((bf16[128,320]{1,0:T(8,128)(2,1)S(1)}, bf16[128,320]{1,0:T(8,128)(2,1)S(1)}, u32[]{:S(2)}, u32[]{:S(2)}) %collective-permute-start.6) | collective-permute-done | bytes 81952 | tf_op jit(solution)/shard_map/ppermute | solution.py:394
  122.0 2.4 %collective-permute-start.7 = (bf16[256,320]{1,0:T(8,128)(2,1)S(1)}, bf16[256,320]{1,0:T(8,128)(2,1)S(1)}, u32[]{:S(2)}, u32[]{:S(2)}) collective-permute-start(bf16[256,320]{1,0:T(8,128)(2,1)S(1)} %get-tuple-element.52), channel_id=1, source_target_pairs={{0,8},{8,16},{16,24},{24,32},{32,40},{40,48},{48,56},{56,64},{64,7... | collective-permute-start | bytes 491528 | tf_op jit(solution)/shard_map/ppermute | solution.py:403
  124.5 4.1 %collective-permute-start.8 = (bf16[256,320]{1,0:T(8,128)(2,1)S(1)}, bf16[256,320]{1,0:T(8,128)(2,1)S(1)}, u32[]{:S(2)}, u32[]{:S(2)}) collective-permute-start(bf16[256,320]{1,0:T(8,128)(2,1)S(1)} %get-tuple-element.53), channel_id=1, source_target_pairs={{0,248},{8,0},{16,8},{24,16},{32,24},{40,32},{48,40},{56,48},{64,5... | collective-permute-start | bytes 491528 | tf_op jit(solution)/shard_map/ppermute | solution.py:404
  128.6 9.6 %collective-permute-start.13 = (bf16[512,320]{1,0:T(8,128)(2,1)S(1)}, bf16[512,320]{1,0:T(8,128)(2,1)S(1)}, u32[]{:S(2)}, u32[]{:S(2)}) collective-permute-start(bf16[512,320]{1,0:T(8,128)(2,1)S(1)} %get-tuple-element.54.refs_4_), channel_id=1, source_target_pairs={{0,4},{4,0},{1,5},{5,1},{2,6},{6,2},{3,7},{7,3},{8,12},{12,8},{9,1... | collective-permute-start | bytes 983048 | tf_op jit(solution)/shard_map/ppermute | solution.py:406
  138.3 2.7 %attend.7 = (f32[512,128]{1,0:T(8,128)S(1)}, f32[512,256]{1,0:T(8,128)S(1)}, f32[512,128]{1,0:T(8,128)S(1)}, f32[512,256]{1,0:T(8,128)S(1)}, f32[512,128]{1,0:T(...) custom-call(bf16[512,320]{1,0:T(8,128)(2,1)S(1)} %collective-permute-done.9.refs_0_, ...), custom_call_target="tpu_custom_call" | custom-call | flops 1207959552 | bytes 5832704 | tf_op jit(solution)/shard_map/attend/pallas_call | solution.py:128
  141.0 2.1 %collective-permute-start.12 = (bf16[512,320]{1,0:T(8,128)(2,1)S(1)}, bf16[512,320]{1,0:T(8,128)(2,1)S(1)}, u32[]{:S(2)}, u32[]{:S(2)}) collective-permute-start(bf16[512,320]{1,0:T(8,128)(2,1)S(1)} %assemble.7.refs_4_), channel_id=1, source_target_pairs={{0,4},{4,0},{1,5},{5,1},{2,6},{6,2},{3,7},{7,3},{8,12},{12,8},{9,1... | collective-permute-start | bytes 983048 | tf_op jit(solution)/shard_map/ppermute | solution.py:411
  143.2 3.4 %attend.8 = (f32[512,128]{1,0:T(8,128)S(1)}, f32[512,256]{1,0:T(8,128)S(1)}, f32[512,128]{1,0:T(8,128)S(1)}, f32[512,256]{1,0:T(8,128)S(1)}, f32[512,128]{1,0:T(...) custom-call(bf16[512,320]{1,0:T(8,128)(2,1)S(1)} %collective-permute-done.9.refs_0_, ...), custom_call_target="tpu_custom_call" | custom-call | flops 1207959552 | bytes 5832704 | tf_op jit(solution)/shard_map/attend/pallas_call | solution.py:128
  146.6 3.4 %attend.9 = (f32[512,128]{1,0:T(8,128)S(1)}, f32[512,256]{1,0:T(8,128)S(1)}, f32[512,128]{1,0:T(8,128)S(1)}, f32[512,256]{1,0:T(8,128)S(1)}, f32[512,128]{1,0:T(...) custom-call(bf16[512,320]{1,0:T(8,128)(2,1)S(1)} %collective-permute-done.9.refs_0_, ...), custom_call_target="tpu_custom_call" | custom-call | flops 1207959552 | bytes 5832704 | tf_op jit(solution)/shard_map/attend/pallas_call | solution.py:128
  151.5 2.2 %collective-permute-start.16 = (bf16[528,256]{1,0:T(8,128)(2,1)S(1)}, bf16[528,256]{1,0:T(8,128)(2,1)S(1)}, u32[]{:S(2)}, u32[]{:S(2)}) collective-permute-start(bf16[528,256]{1,0:T(8,128)(2,1)S(1)} %attend.13), channel_id=1, source_target_pairs={{0,1},{1,2},{2,3},{3,0},{4,5},{5,6},{6,7},{7,4},{8,9},{9,10},{10,1... | collective-permute-start | bytes 811016 | tf_op jit(solution)/shard_map/ppermute | solution.py:417
  155.3 4.3 %collective-permute-start.15 = (bf16[528,256]{1,0:T(8,128)(2,1)S(1)}, bf16[528,256]{1,0:T(8,128)(2,1)S(1)}, u32[]{:S(2)}, u32[]{:S(2)}) collective-permute-start(bf16[528,256]{1,0:T(8,128)(2,1)S(1)} %attend.12), channel_id=1, source_target_pairs={{0,3},{1,0},{2,1},{3,2},{4,7},{5,4},{6,5},{7,6},{8,11},{9,8},{10,9... | collective-permute-start | bytes 811016 | tf_op jit(solution)/shard_map/ppermute | solution.py:417
  161.2 2.3 %collective-permute-start.14 = (bf16[528,256]{1,0:T(8,128)(2,1)S(1)}, bf16[528,256]{1,0:T(8,128)(2,1)S(1)}, u32[]{:S(2)}, u32[]{:S(2)}) collective-permute-start(bf16[528,256]{1,0:T(8,128)(2,1)S(1)} %attend.11), channel_id=1, source_target_pairs={{0,2},{1,3},{2,0},{3,1},{4,6},{5,7},{6,4},{7,5},{8,10},{9,11},{10,... | collective-permute-start | bytes 811016 | tf_op jit(solution)/shard_map/ppermute | solution.py:417
  164.8 6.9 %collective-permute-done.14.refs_0_ = bf16[528,256]{1,0:T(8,128)(2,1)S(1)} collective-permute-done((bf16[528,256]{1,0:T(8,128)(2,1)S(1)}, bf16[528,256]{1,0:T(8,128)(2,1)S(1)}, u32[]{:S(2)}, u32[]{:S(2)}) %collective-permute-start.14) | collective-permute-done | bytes 270368 | tf_op jit(solution)/shard_map/ppermute | solution.py:417
  173.5 12.2 %all-gather = bf16[512,640]{1,0:T(8,128)(2,1)} all-gather(bf16[128,640]{1,0:T(8,128)(2,1)S(1)} %combine.1), channel_id=2, replica_groups=mesh['grp'=2,'z'=32,'core'=2,'tp'=4] {'tp'}, dimensions={0}, use_global_device_ids=true | all-gather | bytes 819200 | tf_op jit(solution)/shard_map/all_gather | solution.py:420
  185.7 3.4 %project.1 = bf16[128,1024]{1,0:T(8,128)(2,1)} custom-call(bf16[4,128,640]{2,1,0:T(8,128)(2,1)} %bitcast.24, bf16[2048,1024]{1,0:T(8,128)(2,1)} %all-gather.3.cloned.1.call-done.weight_hbm), custom_call_target="tpu_custom_call" | custom-call | flops 536870912 | bytes 4194304 | tf_op jit(solution)/shard_map/project/pallas_call | solution.py:313
  (58 shorter events, 16.1 us)
Async XLA Ops:
  6.5 1.8 copy-start
  6.6 179.2 %all-gather.3.cloned.1.call-start = ((), (), s32[]{:S(2)}) async-start(), calls=%async_computation | async-start | bytes 4259840 | tf_op jit(solution)/shard_map/all_gather | solution.py:358
  10.4 12.0 %copy-start.2 = (bf16[32,256]{1,0:T(8,128)(2,1)S(1)}, bf16[32,256]{1,0:T(8,128)(2,1)}, u32[]{:S(2)}) copy-start(bf16[32,256]{1,0:T(8,128)(2,1)} %latent_hbm.1) | copy-start | bytes 49156
  10.4 12.0 %copy-start.3 = (bf16[32,64]{1,0:T(8,128)(2,1)S(1)}, bf16[32,64]{1,0:T(8,128)(2,1)}, u32[]{:S(2)}) copy-start(bf16[32,64]{1,0:T(8,128)(2,1)} %rotary_hbm.1) | copy-start | bytes 12292
  10.4 12.0 %copy-start.5 = (f32[256]{0:T(256)S(1)}, f32[256]{0:T(256)}, u32[]{:S(2)}) copy-start(f32[256]{0:T(256)} %param.14) | copy-start | bytes 3076
  11.1 117.5 %collective-permute-start.10 = (bf16[512,320]{1,0:T(8,128)(2,1)S(1)}, bf16[512,320]{1,0:T(8,128)(2,1)S(1)}, u32[]{:S(2)}, u32[]{:S(2)}) collective-permute-start(bf16[512,320]{1,0:T(8,128)(2,1)S(1)} %bitcast.15), channel_id=1, source_target_pairs={{0,1},{1,2},{2,3},{3,0},{4,5},{5,6},{6,7},{7,4},{8,9},{9,10},{10,1... | collective-permute-start | bytes 983048 | tf_op jit(solution)/shard_map/ppermute | solution.py:386
  15.2 123.0 %collective-permute-start.11 = (bf16[512,320]{1,0:T(8,128)(2,1)S(1)}, bf16[512,320]{1,0:T(8,128)(2,1)S(1)}, u32[]{:S(2)}, u32[]{:S(2)}) collective-permute-start(bf16[512,320]{1,0:T(8,128)(2,1)S(1)} %bitcast.16), channel_id=1, source_target_pairs={{0,3},{1,0},{2,1},{3,2},{4,7},{5,4},{6,5},{7,6},{8,11},{9,8},{10,9... | collective-permute-start | bytes 983048 | tf_op jit(solution)/shard_map/ppermute | solution.py:386
  18.7 119.5 %collective-permute-start.9 = (bf16[512,320]{1,0:T(8,128)(2,1)S(1)}, bf16[512,320]{1,0:T(8,128)(2,1)S(1)}, u32[]{:S(2)}, u32[]{:S(2)}) collective-permute-start(bf16[512,320]{1,0:T(8,128)(2,1)S(1)} %bitcast.17), channel_id=1, source_target_pairs={{0,2},{1,3},{2,0},{3,1},{4,6},{5,7},{6,4},{7,5},{8,10},{9,11},{10,... | collective-permute-start | bytes 983048 | tf_op jit(solution)/shard_map/ppermute | solution.py:386
  22.7 55.2 %collective-permute-start = (bf16[32,320]{1,0:T(8,128)(2,1)S(1)}, bf16[32,320]{1,0:T(8,128)(2,1)S(1)}, u32[]{:S(2)}, u32[]{:S(2)}) collective-permute-start(bf16[32,320]{1,0:T(8,128)(2,1)S(1)} %prepare.1.refs_0_), channel_id=1, source_target_pairs={{0,128},{8,136},{16,144},{24,152},{32,160},{40,168},{48,176},{56,1... | collective-permute-start | bytes 61448 | tf_op jit(solution)/shard_map/ppermute | solution.py:365
  65.2 25.1 %collective-permute-start.1 = (bf16[32,320]{1,0:T(8,128)(2,1)S(1)}, bf16[32,320]{1,0:T(8,128)(2,1)S(1)}, u32[]{:S(2)}, u32[]{:S(2)}) collective-permute-start(bf16[32,320]{1,0:T(8,128)(2,1)S(1)} %prepare.1.refs_0_), channel_id=1, source_target_pairs={{0,64},{8,72},{16,80},{24,88},{32,96},{40,104},{48,112},{56,120},{... | collective-permute-start | bytes 61448 | tf_op jit(solution)/shard_map/ppermute | solution.py:365
  77.9 13.5 %collective-permute-start.2 = (bf16[32,320]{1,0:T(8,128)(2,1)S(1)}, bf16[32,320]{1,0:T(8,128)(2,1)S(1)}, u32[]{:S(2)}, u32[]{:S(2)}) collective-permute-start(bf16[32,320]{1,0:T(8,128)(2,1)S(1)} %prepare.1.refs_0_), channel_id=1, source_target_pairs={{0,192},{8,200},{16,208},{24,216},{32,224},{40,232},{48,240},{56,2... | collective-permute-start | bytes 61448 | tf_op jit(solution)/shard_map/ppermute | solution.py:365
  91.4 14.8 %collective-permute-start.3 = (bf16[64,320]{1,0:T(8,128)(2,1)S(1)}, bf16[64,320]{1,0:T(8,128)(2,1)S(1)}, u32[]{:S(2)}, u32[]{:S(2)}) collective-permute-start(bf16[64,320]{1,0:T(8,128)(2,1)S(1)} %get-tuple-element.48.refs_0_), channel_id=1, source_target_pairs={{0,32},{8,40},{16,48},{24,56},{32,64},{40,72},{48,80},{56,88},{64,... | collective-permute-start | bytes 122888 | tf_op jit(solution)/shard_map/ppermute | solution.py:393
  98.9 8.8 %collective-permute-start.4 = (bf16[64,320]{1,0:T(8,128)(2,1)S(1)}, bf16[64,320]{1,0:T(8,128)(2,1)S(1)}, u32[]{:S(2)}, u32[]{:S(2)}) collective-permute-start(bf16[64,320]{1,0:T(8,128)(2,1)S(1)} %get-tuple-element.49.refs_2_), channel_id=1, source_target_pairs={{0,224},{8,232},{16,240},{24,248},{32,0},{40,8},{48,16},{56,24},{6... | collective-permute-start | bytes 122888 | tf_op jit(solution)/shard_map/ppermute | solution.py:394
  107.8 11.8 %collective-permute-start.5 = (bf16[128,320]{1,0:T(8,128)(2,1)S(1)}, bf16[128,320]{1,0:T(8,128)(2,1)S(1)}, u32[]{:S(2)}, u32[]{:S(2)}) collective-permute-start(bf16[128,320]{1,0:T(8,128)(2,1)S(1)} %get-tuple-element.50.refs_0_), channel_id=1, source_target_pairs={{0,16},{8,24},{16,32},{24,40},{32,48},{40,56},{48,64},{56,72},{64,... | collective-permute-start | bytes 245768 | tf_op jit(solution)/shard_map/ppermute | solution.py:393
  113.0 9.0 %collective-permute-start.6 = (bf16[128,320]{1,0:T(8,128)(2,1)S(1)}, bf16[128,320]{1,0:T(8,128)(2,1)S(1)}, u32[]{:S(2)}, u32[]{:S(2)}) collective-permute-start(bf16[128,320]{1,0:T(8,128)(2,1)S(1)} %get-tuple-element.51.refs_2_), channel_id=1, source_target_pairs={{0,240},{8,248},{16,0},{24,8},{32,16},{40,24},{48,32},{56,40},{64,... | collective-permute-start | bytes 245768 | tf_op jit(solution)/shard_map/ppermute | solution.py:394
  122.0 18.9 %collective-permute-start.7 = (bf16[256,320]{1,0:T(8,128)(2,1)S(1)}, bf16[256,320]{1,0:T(8,128)(2,1)S(1)}, u32[]{:S(2)}, u32[]{:S(2)}) collective-permute-start(bf16[256,320]{1,0:T(8,128)(2,1)S(1)} %get-tuple-element.52), channel_id=1, source_target_pairs={{0,8},{8,16},{16,24},{24,32},{32,40},{40,48},{48,56},{56,64},{64,7... | collective-permute-start | bytes 491528 | tf_op jit(solution)/shard_map/ppermute | solution.py:403
  124.5 16.5 %collective-permute-start.8 = (bf16[256,320]{1,0:T(8,128)(2,1)S(1)}, bf16[256,320]{1,0:T(8,128)(2,1)S(1)}, u32[]{:S(2)}, u32[]{:S(2)}) collective-permute-start(bf16[256,320]{1,0:T(8,128)(2,1)S(1)} %get-tuple-element.53), channel_id=1, source_target_pairs={{0,248},{8,0},{16,8},{24,16},{32,24},{40,32},{48,40},{56,48},{64,5... | collective-permute-start | bytes 491528 | tf_op jit(solution)/shard_map/ppermute | solution.py:404
  128.6 17.9 %collective-permute-start.13 = (bf16[512,320]{1,0:T(8,128)(2,1)S(1)}, bf16[512,320]{1,0:T(8,128)(2,1)S(1)}, u32[]{:S(2)}, u32[]{:S(2)}) collective-permute-start(bf16[512,320]{1,0:T(8,128)(2,1)S(1)} %get-tuple-element.54.refs_4_), channel_id=1, source_target_pairs={{0,4},{4,0},{1,5},{5,1},{2,6},{6,2},{3,7},{7,3},{8,12},{12,8},{9,1... | collective-permute-start | bytes 983048 | tf_op jit(solution)/shard_map/ppermute | solution.py:406
  141.0 9.0 %collective-permute-start.12 = (bf16[512,320]{1,0:T(8,128)(2,1)S(1)}, bf16[512,320]{1,0:T(8,128)(2,1)S(1)}, u32[]{:S(2)}, u32[]{:S(2)}) collective-permute-start(bf16[512,320]{1,0:T(8,128)(2,1)S(1)} %assemble.7.refs_4_), channel_id=1, source_target_pairs={{0,4},{4,0},{1,5},{5,1},{2,6},{6,2},{3,7},{7,3},{8,12},{12,8},{9,1... | collective-permute-start | bytes 983048 | tf_op jit(solution)/shard_map/ppermute | solution.py:411
  151.5 13.3 %collective-permute-start.16 = (bf16[528,256]{1,0:T(8,128)(2,1)S(1)}, bf16[528,256]{1,0:T(8,128)(2,1)S(1)}, u32[]{:S(2)}, u32[]{:S(2)}) collective-permute-start(bf16[528,256]{1,0:T(8,128)(2,1)S(1)} %attend.13), channel_id=1, source_target_pairs={{0,1},{1,2},{2,3},{3,0},{4,5},{5,6},{6,7},{7,4},{8,9},{9,10},{10,1... | collective-permute-start | bytes 811016 | tf_op jit(solution)/shard_map/ppermute | solution.py:417
  155.3 9.5 %collective-permute-start.15 = (bf16[528,256]{1,0:T(8,128)(2,1)S(1)}, bf16[528,256]{1,0:T(8,128)(2,1)S(1)}, u32[]{:S(2)}, u32[]{:S(2)}) collective-permute-start(bf16[528,256]{1,0:T(8,128)(2,1)S(1)} %attend.12), channel_id=1, source_target_pairs={{0,3},{1,0},{2,1},{3,2},{4,7},{5,4},{6,5},{7,6},{8,11},{9,8},{10,9... | collective-permute-start | bytes 811016 | tf_op jit(solution)/shard_map/ppermute | solution.py:417
  161.2 10.6 %copy-start.1 = (bf16[256,512]{1,0:T(8,128)(2,1)S(1)}, bf16[256,512]{1,0:T(8,128)(2,1)}, u32[]{:S(2)}) copy-start(bf16[256,512]{1,0:T(8,128)(2,1)} %refs_3_.1) | copy-start | bytes 786436
  161.2 10.6 %copy-start.4 = (f32[512]{0:T(512)S(1)}, f32[512]{0:T(512)}, u32[]{:S(2)}) copy-start(f32[512]{0:T(512)} %param.18) | copy-start | bytes 6148
  161.2 10.5 %collective-permute-start.14 = (bf16[528,256]{1,0:T(8,128)(2,1)S(1)}, bf16[528,256]{1,0:T(8,128)(2,1)S(1)}, u32[]{:S(2)}, u32[]{:S(2)}) collective-permute-start(bf16[528,256]{1,0:T(8,128)(2,1)S(1)} %attend.11), channel_id=1, source_target_pairs={{0,2},{1,3},{2,0},{3,1},{4,6},{5,7},{6,4},{7,5},{8,10},{9,11},{10,... | collective-permute-start | bytes 811016 | tf_op jit(solution)/shard_map/ppermute | solution.py:417
  (1 other events, 1.0 us)
Sparse Core Ops, SparseCore 0:
  9.5 167.8 all-gather.2

commit v3 on v2

--- a/solution.py
+++ b/solution.py
@@ -272,54 +272,70 @@
 
 
 def project_kernel(
-    blocks, everyone_hbm, weight_hbm, out_ref, everyone_ref, weight_ref, total, sems
+    blocks, halves, everyone_hbm, weight_hbm, out_ref, everyone_ref, weight_ref, total, sems
 ):
-    depth = weight_ref.shape[0] // blocks
+    step = pl.program_id(0)
+    depth = weight_ref.shape[1] // blocks
+    part = weight_ref.shape[2]
     sides, _, width = everyone_ref.shape
     width -= 128
     shared = width // depth
-    activations = pltpu.make_async_copy(everyone_hbm, everyone_ref, sems.at[blocks])
-    activations.start()
-    copies = []
-    for block in range(blocks):
+    activations = pltpu.make_async_copy(everyone_hbm, everyone_ref, sems.at[halves, 0])
+
+    def weights(half, block):
         span = pl.ds(block * depth, depth)
-        copies.append(
-            pltpu.make_async_copy(weight_hbm.at[span, :], weight_ref.at[span, :], sems.at[block])
+        return pltpu.make_async_copy(
+            weight_hbm.at[span, pl.ds(half * part, part)],
+            weight_ref.at[half, span, :],
+            sems.at[half, block],
         )
-        copies[-1].start()
-    activations.wait()
+
+    @pl.when(step == 0)
+    def _():
+        activations.start()
+        for half in range(halves):
+            for block in range(blocks):
+                weights(half, block).start()
+        activations.wait()
+
     squares = sum(
         everyone_ref[side, :, pl.ds(width, 128)].astype(jnp.float32) for side in range(sides)
     )
     scale = lax.rsqrt(squares[:, :1] / (HEADS * VALUE_DIM) + norm_eps)
-    for block in range(blocks):
-        copies[block].wait()
-        product = jnp.dot(
-            everyone_ref[block // shared, :, pl.ds(block % shared * depth, depth)],
-            weight_ref[pl.ds(block * depth, depth), :],
-            preferred_element_type=jnp.float32,
-        )
-        if block == 0:
-            total[...] = product
-        elif block < blocks - 1:
-            total[...] += product
-        else:
-            out_ref[...] = ((total[...] + product) * scale).astype(jnp.bfloat16)
-
-
-def project(everyone, weight, blocks=8):
+    for half in range(halves):
+
+        @pl.when(step == half)
+        def _():
+            for block in range(blocks):
+                weights(half, block).wait()
+                product = jnp.dot(
+                    everyone_ref[block // shared, :, pl.ds(block % shared * depth, depth)],
+                    weight_ref[half, pl.ds(block * depth, depth), :],
+                    preferred_element_type=jnp.float32,
+                )
+                if block == 0:
+                    total[...] = product
+                elif block < blocks - 1:
+                    total[...] += product
+                else:
+                    out_ref[...] = ((total[...] + product) * scale).astype(jnp.bfloat16)
+
+
+def project(everyone, weight, blocks=4, halves=2):
     tokens = everyone.shape[1]
     depth, features = weight.shape
+    part = features // halves
     return pl.pallas_call(
-        functools.partial(project_kernel, blocks),
+        functools.partial(project_kernel, blocks, halves),
+        grid=(halves,),
         out_shape=jax.ShapeDtypeStruct((tokens, features), jnp.bfloat16),
         in_specs=[pl.BlockSpec(memory_space=pltpu.HBM)] * 2,
-        out_specs=pl.BlockSpec(memory_space=pltpu.VMEM),
+        out_specs=pl.BlockSpec((tokens, part), lambda step: (0, step)),
         scratch_shapes=[
             pltpu.VMEM(everyone.shape, everyone.dtype),
-            pltpu.VMEM(weight.shape, weight.dtype),
-            pltpu.VMEM((tokens, features), jnp.float32),
-            pltpu.SemaphoreType.DMA((blocks + 1,)),
+            pltpu.VMEM((halves, depth, part), weight.dtype),
+            pltpu.VMEM((tokens, part), jnp.float32),
+            pltpu.SemaphoreType.DMA((halves + 1, blocks)),
         ],
         cost_estimate=pl.CostEstimate(
             flops=2 * tokens * depth * features,

time: 199 us -> 199 us (level)
  no operation moved by 1% of the time
where the time goes in v3:
time: 199 us; the launch traced here: 196 us
  starting transfers between devices  132 us (66%)
  Pallas kernels  21 us (11%)
  between operations  13.9 us (7%)
  waiting for transfers between devices  13.5 us (7%)
  blocking collectives  12.2 us (6%)
    ppermute x3, starting transfers between devices, on_device(): others.append(lax.ppermute(own, 'z', shifted(chips, by)))  67.5 us
    pallas_call x7, Pallas kernels, attend(): pl.pallas_call(functools.partial(attend_kernel, guests, not state, last,...  15.4 us
    ppermute x2, starting transfers between devices, on_device(): down_next = lax.ppermute(down, 'z', shifted(chips, -distance))  13.1 us
    ppermute x2, starting transfers between devices, on_device(): up_next = lax.ppermute(up, 'z', shifted(chips, distance))  12.7 us
    all_gather x1, blocking collectives, on_device(): everyone = lax.all_gather(sent, 'tp', axis=0)  12.2 us
    ppermute x3, starting transfers between devices, on_device(): guests.append(lax.ppermute(queries, 'tp', shifted(sides, by)))  11.1 us
    ppermute x1, starting transfers between devices, on_device(): partner_near = lax.ppermute(near, 'core', swap)  9.61 us
    ppermute x3, starting transfers between devices, on_device(): parts.append(lax.ppermute(part, 'tp', shifted(sides, -by)))  8.86 us
  transfers between devices with their start and end apart: 18, of which 5 were waited for; matrix products, arithmetic and copies ran while one was open for 2% of the time, Pallas kernels for 9%

profile of v3, /device:TPU:33, one launch (start us, length us, event | category | flops | bytes accessed | tf_op | source)
XLA Modules:
  0.0 196.2 jit_solution(4883068968894025042)
XLA Ops:
  11.1 4.1 %collective-permute-start.10 = (bf16[512,320]{1,0:T(8,128)(2,1)S(1)}, bf16[512,320]{1,0:T(8,128)(2,1)S(1)}, u32[]{:S(2)}, u32[]{:S(2)}) collective-permute-start(bf16[512,320]{1,0:T(8,128)(2,1)S(1)} %bitcast.15), channel_id=1, source_target_pairs={{0,1},{1,2},{2,3},{3,0},{4,5},{5,6},{6,7},{7,4},{8,9},{9,10},{10,1... | collective-permute-start | bytes 983048 | tf_op jit(solution)/shard_map/ppermute | solution.py:402
  15.2 3.5 %collective-permute-start.11 = (bf16[512,320]{1,0:T(8,128)(2,1)S(1)}, bf16[512,320]{1,0:T(8,128)(2,1)S(1)}, u32[]{:S(2)}, u32[]{:S(2)}) collective-permute-start(bf16[512,320]{1,0:T(8,128)(2,1)S(1)} %bitcast.16), channel_id=1, source_target_pairs={{0,3},{1,0},{2,1},{3,2},{4,7},{5,4},{6,5},{7,6},{8,11},{9,8},{10,9... | collective-permute-start | bytes 983048 | tf_op jit(solution)/shard_map/ppermute | solution.py:402
  18.7 3.5 %collective-permute-start.9 = (bf16[512,320]{1,0:T(8,128)(2,1)S(1)}, bf16[512,320]{1,0:T(8,128)(2,1)S(1)}, u32[]{:S(2)}, u32[]{:S(2)}) collective-permute-start(bf16[512,320]{1,0:T(8,128)(2,1)S(1)} %bitcast.17), channel_id=1, source_target_pairs={{0,2},{1,3},{2,0},{3,1},{4,6},{5,7},{6,4},{7,5},{8,10},{9,11},{10,... | collective-permute-start | bytes 983048 | tf_op jit(solution)/shard_map/ppermute | solution.py:402
  22.7 42.5 %collective-permute-start = (bf16[32,320]{1,0:T(8,128)(2,1)S(1)}, bf16[32,320]{1,0:T(8,128)(2,1)S(1)}, u32[]{:S(2)}, u32[]{:S(2)}) collective-permute-start(bf16[32,320]{1,0:T(8,128)(2,1)S(1)} %prepare.1.refs_0_), channel_id=1, source_target_pairs={{0,128},{8,136},{16,144},{24,152},{32,160},{40,168},{48,176},{56,1... | collective-permute-start | bytes 61448 | tf_op jit(solution)/shard_map/ppermute | solution.py:381
  65.2 12.7 %collective-permute-start.1 = (bf16[32,320]{1,0:T(8,128)(2,1)S(1)}, bf16[32,320]{1,0:T(8,128)(2,1)S(1)}, u32[]{:S(2)}, u32[]{:S(2)}) collective-permute-start(bf16[32,320]{1,0:T(8,128)(2,1)S(1)} %prepare.1.refs_0_), channel_id=1, source_target_pairs={{0,64},{8,72},{16,80},{24,88},{32,96},{40,104},{48,112},{56,120},{... | collective-permute-start | bytes 61448 | tf_op jit(solution)/shard_map/ppermute | solution.py:381
  77.9 12.3 %collective-permute-start.2 = (bf16[32,320]{1,0:T(8,128)(2,1)S(1)}, bf16[32,320]{1,0:T(8,128)(2,1)S(1)}, u32[]{:S(2)}, u32[]{:S(2)}) collective-permute-start(bf16[32,320]{1,0:T(8,128)(2,1)S(1)} %prepare.1.refs_0_), channel_id=1, source_target_pairs={{0,192},{8,200},{16,208},{24,216},{32,224},{40,232},{48,240},{56,2... | collective-permute-start | bytes 61448 | tf_op jit(solution)/shard_map/ppermute | solution.py:381
  91.4 7.5 %collective-permute-start.3 = (bf16[64,320]{1,0:T(8,128)(2,1)S(1)}, bf16[64,320]{1,0:T(8,128)(2,1)S(1)}, u32[]{:S(2)}, u32[]{:S(2)}) collective-permute-start(bf16[64,320]{1,0:T(8,128)(2,1)S(1)} %get-tuple-element.48.refs_0_), channel_id=1, source_target_pairs={{0,32},{8,40},{16,48},{24,56},{32,64},{40,72},{48,80},{56,88},{64,... | collective-permute-start | bytes 122888 | tf_op jit(solution)/shard_map/ppermute | solution.py:409
  98.9 7.3 %collective-permute-start.4 = (bf16[64,320]{1,0:T(8,128)(2,1)S(1)}, bf16[64,320]{1,0:T(8,128)(2,1)S(1)}, u32[]{:S(2)}, u32[]{:S(2)}) collective-permute-start(bf16[64,320]{1,0:T(8,128)(2,1)S(1)} %get-tuple-element.49.refs_2_), channel_id=1, source_target_pairs={{0,224},{8,232},{16,240},{24,248},{32,0},{40,8},{48,16},{56,24},{6... | collective-permute-start | bytes 122888 | tf_op jit(solution)/shard_map/ppermute | solution.py:410
  107.8 5.2 %collective-permute-start.5 = (bf16[128,320]{1,0:T(8,128)(2,1)S(1)}, bf16[128,320]{1,0:T(8,128)(2,1)S(1)}, u32[]{:S(2)}, u32[]{:S(2)}) collective-permute-start(bf16[128,320]{1,0:T(8,128)(2,1)S(1)} %get-tuple-element.50.refs_0_), channel_id=1, source_target_pairs={{0,16},{8,24},{16,32},{24,40},{32,48},{40,56},{48,64},{56,72},{64,... | collective-permute-start | bytes 245768 | tf_op jit(solution)/shard_map/ppermute | solution.py:409
  113.0 5.8 %collective-permute-start.6 = (bf16[128,320]{1,0:T(8,128)(2,1)S(1)}, bf16[128,320]{1,0:T(8,128)(2,1)S(1)}, u32[]{:S(2)}, u32[]{:S(2)}) collective-permute-start(bf16[128,320]{1,0:T(8,128)(2,1)S(1)} %get-tuple-element.51.refs_2_), channel_id=1, source_target_pairs={{0,240},{8,248},{16,0},{24,8},{32,16},{40,24},{48,32},{56,40},{64,... | collective-permute-start | bytes 245768 | tf_op jit(solution)/shard_map/ppermute | solution.py:410
  119.6 2.4 %collective-permute-done.6.refs_3_ = bf16[128,320]{1,0:T(8,128)(2,1)S(1)} collective-permute-done((bf16[128,320]{1,0:T(8,128)(2,1)S(1)}, bf16[128,320]{1,0:T(8,128)(2,1)S(1)}, u32[]{:S(2)}, u32[]{:S(2)}) %collective-permute-start.6) | collective-permute-done | bytes 81952 | tf_op jit(solution)/shard_map/ppermute | solution.py:410
  122.0 2.4 %collective-permute-start.7 = (bf16[256,320]{1,0:T(8,128)(2,1)S(1)}, bf16[256,320]{1,0:T(8,128)(2,1)S(1)}, u32[]{:S(2)}, u32[]{:S(2)}) collective-permute-start(bf16[256,320]{1,0:T(8,128)(2,1)S(1)} %get-tuple-element.52), channel_id=1, source_target_pairs={{0,8},{8,16},{16,24},{24,32},{32,40},{40,48},{48,56},{56,64},{64,7... | collective-permute-start | bytes 491528 | tf_op jit(solution)/shard_map/ppermute | solution.py:419
  124.5 4.1 %collective-permute-start.8 = (bf16[256,320]{1,0:T(8,128)(2,1)S(1)}, bf16[256,320]{1,0:T(8,128)(2,1)S(1)}, u32[]{:S(2)}, u32[]{:S(2)}) collective-permute-start(bf16[256,320]{1,0:T(8,128)(2,1)S(1)} %get-tuple-element.53), channel_id=1, source_target_pairs={{0,248},{8,0},{16,8},{24,16},{32,24},{40,32},{48,40},{56,48},{64,5... | collective-permute-start | bytes 491528 | tf_op jit(solution)/shard_map/ppermute | solution.py:420
  128.6 9.6 %collective-permute-start.13 = (bf16[512,320]{1,0:T(8,128)(2,1)S(1)}, bf16[512,320]{1,0:T(8,128)(2,1)S(1)}, u32[]{:S(2)}, u32[]{:S(2)}) collective-permute-start(bf16[512,320]{1,0:T(8,128)(2,1)S(1)} %get-tuple-element.54.refs_4_), channel_id=1, source_target_pairs={{0,4},{4,0},{1,5},{5,1},{2,6},{6,2},{3,7},{7,3},{8,12},{12,8},{9,1... | collective-permute-start | bytes 983048 | tf_op jit(solution)/shard_map/ppermute | solution.py:422
  138.3 2.7 %attend.7 = (f32[512,128]{1,0:T(8,128)S(1)}, f32[512,256]{1,0:T(8,128)S(1)}, f32[512,128]{1,0:T(8,128)S(1)}, f32[512,256]{1,0:T(8,128)S(1)}, f32[512,128]{1,0:T(...) custom-call(bf16[512,320]{1,0:T(8,128)(2,1)S(1)} %collective-permute-done.9.refs_0_, ...), custom_call_target="tpu_custom_call" | custom-call | flops 1207959552 | bytes 5832704 | tf_op jit(solution)/shard_map/attend/pallas_call | solution.py:128
  141.0 2.1 %collective-permute-start.12 = (bf16[512,320]{1,0:T(8,128)(2,1)S(1)}, bf16[512,320]{1,0:T(8,128)(2,1)S(1)}, u32[]{:S(2)}, u32[]{:S(2)}) collective-permute-start(bf16[512,320]{1,0:T(8,128)(2,1)S(1)} %assemble.7.refs_4_), channel_id=1, source_target_pairs={{0,4},{4,0},{1,5},{5,1},{2,6},{6,2},{3,7},{7,3},{8,12},{12,8},{9,1... | collective-permute-start | bytes 983048 | tf_op jit(solution)/shard_map/ppermute | solution.py:427
  143.2 3.4 %attend.8 = (f32[512,128]{1,0:T(8,128)S(1)}, f32[512,256]{1,0:T(8,128)S(1)}, f32[512,128]{1,0:T(8,128)S(1)}, f32[512,256]{1,0:T(8,128)S(1)}, f32[512,128]{1,0:T(...) custom-call(bf16[512,320]{1,0:T(8,128)(2,1)S(1)} %collective-permute-done.9.refs_0_, ...), custom_call_target="tpu_custom_call" | custom-call | flops 1207959552 | bytes 5832704 | tf_op jit(solution)/shard_map/attend/pallas_call | solution.py:128
  146.6 3.4 %attend.9 = (f32[512,128]{1,0:T(8,128)S(1)}, f32[512,256]{1,0:T(8,128)S(1)}, f32[512,128]{1,0:T(8,128)S(1)}, f32[512,256]{1,0:T(8,128)S(1)}, f32[512,128]{1,0:T(...) custom-call(bf16[512,320]{1,0:T(8,128)(2,1)S(1)} %collective-permute-done.9.refs_0_, ...), custom_call_target="tpu_custom_call" | custom-call | flops 1207959552 | bytes 5832704 | tf_op jit(solution)/shard_map/attend/pallas_call | solution.py:128
  151.5 2.2 %collective-permute-start.16 = (bf16[528,256]{1,0:T(8,128)(2,1)S(1)}, bf16[528,256]{1,0:T(8,128)(2,1)S(1)}, u32[]{:S(2)}, u32[]{:S(2)}) collective-permute-start(bf16[528,256]{1,0:T(8,128)(2,1)S(1)} %attend.13), channel_id=1, source_target_pairs={{0,1},{1,2},{2,3},{3,0},{4,5},{5,6},{6,7},{7,4},{8,9},{9,10},{10,1... | collective-permute-start | bytes 811016 | tf_op jit(solution)/shard_map/ppermute | solution.py:433
  155.3 4.3 %collective-permute-start.15 = (bf16[528,256]{1,0:T(8,128)(2,1)S(1)}, bf16[528,256]{1,0:T(8,128)(2,1)S(1)}, u32[]{:S(2)}, u32[]{:S(2)}) collective-permute-start(bf16[528,256]{1,0:T(8,128)(2,1)S(1)} %attend.12), channel_id=1, source_target_pairs={{0,3},{1,0},{2,1},{3,2},{4,7},{5,4},{6,5},{7,6},{8,11},{9,8},{10,9... | collective-permute-start | bytes 811016 | tf_op jit(solution)/shard_map/ppermute | solution.py:433
  161.2 2.3 %collective-permute-start.14 = (bf16[528,256]{1,0:T(8,128)(2,1)S(1)}, bf16[528,256]{1,0:T(8,128)(2,1)S(1)}, u32[]{:S(2)}, u32[]{:S(2)}) collective-permute-start(bf16[528,256]{1,0:T(8,128)(2,1)S(1)} %attend.11), channel_id=1, source_target_pairs={{0,2},{1,3},{2,0},{3,1},{4,6},{5,7},{6,4},{7,5},{8,10},{9,11},{10,... | collective-permute-start | bytes 811016 | tf_op jit(solution)/shard_map/ppermute | solution.py:433
  164.8 6.9 %collective-permute-done.14.refs_0_ = bf16[528,256]{1,0:T(8,128)(2,1)S(1)} collective-permute-done((bf16[528,256]{1,0:T(8,128)(2,1)S(1)}, bf16[528,256]{1,0:T(8,128)(2,1)S(1)}, u32[]{:S(2)}, u32[]{:S(2)}) %collective-permute-start.14) | collective-permute-done | bytes 270368 | tf_op jit(solution)/shard_map/ppermute | solution.py:433
  173.5 12.2 %all-gather = bf16[512,640]{1,0:T(8,128)(2,1)} all-gather(bf16[128,640]{1,0:T(8,128)(2,1)S(1)} %combine.1), channel_id=2, replica_groups=mesh['grp'=2,'z'=32,'core'=2,'tp'=4] {'tp'}, dimensions={0}, use_global_device_ids=true | all-gather | bytes 819200 | tf_op jit(solution)/shard_map/all_gather | solution.py:436
  185.7 3.6 %project.1 = bf16[128,1024]{1,0:T(8,128)(2,1)} custom-call(bf16[4,128,640]{2,1,0:T(8,128)(2,1)} %bitcast.24, bf16[2048,1024]{1,0:T(8,128)(2,1)} %all-gather.3.cloned.1.call-done.weight_hbm), custom_call_target="tpu_custom_call" | custom-call | flops 536870912 | bytes 4194304 | tf_op jit(solution)/shard_map/project/pallas_call | solution.py:328
  (58 shorter events, 16.1 us)
Async XLA Ops:
  6.5 1.8 copy-start
  6.6 179.2 %all-gather.3.cloned.1.call-start = ((), (), s32[]{:S(2)}) async-start(), calls=%async_computation | async-start | bytes 4259840 | tf_op jit(solution)/shard_map/all_gather | solution.py:374
  10.4 12.0 %copy-start.2 = (bf16[32,256]{1,0:T(8,128)(2,1)S(1)}, bf16[32,256]{1,0:T(8,128)(2,1)}, u32[]{:S(2)}) copy-start(bf16[32,256]{1,0:T(8,128)(2,1)} %latent_hbm.1) | copy-start | bytes 49156
  10.4 12.0 %copy-start.3 = (bf16[32,64]{1,0:T(8,128)(2,1)S(1)}, bf16[32,64]{1,0:T(8,128)(2,1)}, u32[]{:S(2)}) copy-start(bf16[32,64]{1,0:T(8,128)(2,1)} %rotary_hbm.1) | copy-start | bytes 12292
  10.4 12.0 %copy-start.5 = (f32[256]{0:T(256)S(1)}, f32[256]{0:T(256)}, u32[]{:S(2)}) copy-start(f32[256]{0:T(256)} %param.14) | copy-start | bytes 3076
  11.1 117.5 %collective-permute-start.10 = (bf16[512,320]{1,0:T(8,128)(2,1)S(1)}, bf16[512,320]{1,0:T(8,128)(2,1)S(1)}, u32[]{:S(2)}, u32[]{:S(2)}) collective-permute-start(bf16[512,320]{1,0:T(8,128)(2,1)S(1)} %bitcast.15), channel_id=1, source_target_pairs={{0,1},{1,2},{2,3},{3,0},{4,5},{5,6},{6,7},{7,4},{8,9},{9,10},{10,1... | collective-permute-start | bytes 983048 | tf_op jit(solution)/shard_map/ppermute | solution.py:402
  15.2 123.0 %collective-permute-start.11 = (bf16[512,320]{1,0:T(8,128)(2,1)S(1)}, bf16[512,320]{1,0:T(8,128)(2,1)S(1)}, u32[]{:S(2)}, u32[]{:S(2)}) collective-permute-start(bf16[512,320]{1,0:T(8,128)(2,1)S(1)} %bitcast.16), channel_id=1, source_target_pairs={{0,3},{1,0},{2,1},{3,2},{4,7},{5,4},{6,5},{7,6},{8,11},{9,8},{10,9... | collective-permute-start | bytes 983048 | tf_op jit(solution)/shard_map/ppermute | solution.py:402
  18.7 119.5 %collective-permute-start.9 = (bf16[512,320]{1,0:T(8,128)(2,1)S(1)}, bf16[512,320]{1,0:T(8,128)(2,1)S(1)}, u32[]{:S(2)}, u32[]{:S(2)}) collective-permute-start(bf16[512,320]{1,0:T(8,128)(2,1)S(1)} %bitcast.17), channel_id=1, source_target_pairs={{0,2},{1,3},{2,0},{3,1},{4,6},{5,7},{6,4},{7,5},{8,10},{9,11},{10,... | collective-permute-start | bytes 983048 | tf_op jit(solution)/shard_map/ppermute | solution.py:402
  22.7 55.2 %collective-permute-start = (bf16[32,320]{1,0:T(8,128)(2,1)S(1)}, bf16[32,320]{1,0:T(8,128)(2,1)S(1)}, u32[]{:S(2)}, u32[]{:S(2)}) collective-permute-start(bf16[32,320]{1,0:T(8,128)(2,1)S(1)} %prepare.1.refs_0_), channel_id=1, source_target_pairs={{0,128},{8,136},{16,144},{24,152},{32,160},{40,168},{48,176},{56,1... | collective-permute-start | bytes 61448 | tf_op jit(solution)/shard_map/ppermute | solution.py:381
  65.2 25.1 %collective-permute-start.1 = (bf16[32,320]{1,0:T(8,128)(2,1)S(1)}, bf16[32,320]{1,0:T(8,128)(2,1)S(1)}, u32[]{:S(2)}, u32[]{:S(2)}) collective-permute-start(bf16[32,320]{1,0:T(8,128)(2,1)S(1)} %prepare.1.refs_0_), channel_id=1, source_target_pairs={{0,64},{8,72},{16,80},{24,88},{32,96},{40,104},{48,112},{56,120},{... | collective-permute-start | bytes 61448 | tf_op jit(solution)/shard_map/ppermute | solution.py:381
  77.9 13.5 %collective-permute-start.2 = (bf16[32,320]{1,0:T(8,128)(2,1)S(1)}, bf16[32,320]{1,0:T(8,128)(2,1)S(1)}, u32[]{:S(2)}, u32[]{:S(2)}) collective-permute-start(bf16[32,320]{1,0:T(8,128)(2,1)S(1)} %prepare.1.refs_0_), channel_id=1, source_target_pairs={{0,192},{8,200},{16,208},{24,216},{32,224},{40,232},{48,240},{56,2... | collective-permute-start | bytes 61448 | tf_op jit(solution)/shard_map/ppermute | solution.py:381
  91.4 14.8 %collective-permute-start.3 = (bf16[64,320]{1,0:T(8,128)(2,1)S(1)}, bf16[64,320]{1,0:T(8,128)(2,1)S(1)}, u32[]{:S(2)}, u32[]{:S(2)}) collective-permute-start(bf16[64,320]{1,0:T(8,128)(2,1)S(1)} %get-tuple-element.48.refs_0_), channel_id=1, source_target_pairs={{0,32},{8,40},{16,48},{24,56},{32,64},{40,72},{48,80},{56,88},{64,... | collective-permute-start | bytes 122888 | tf_op jit(solution)/shard_map/ppermute | solution.py:409
  98.9 8.8 %collective-permute-start.4 = (bf16[64,320]{1,0:T(8,128)(2,1)S(1)}, bf16[64,320]{1,0:T(8,128)(2,1)S(1)}, u32[]{:S(2)}, u32[]{:S(2)}) collective-permute-start(bf16[64,320]{1,0:T(8,128)(2,1)S(1)} %get-tuple-element.49.refs_2_), channel_id=1, source_target_pairs={{0,224},{8,232},{16,240},{24,248},{32,0},{40,8},{48,16},{56,24},{6... | collective-permute-start | bytes 122888 | tf_op jit(solution)/shard_map/ppermute | solution.py:410
  107.8 11.8 %collective-permute-start.5 = (bf16[128,320]{1,0:T(8,128)(2,1)S(1)}, bf16[128,320]{1,0:T(8,128)(2,1)S(1)}, u32[]{:S(2)}, u32[]{:S(2)}) collective-permute-start(bf16[128,320]{1,0:T(8,128)(2,1)S(1)} %get-tuple-element.50.refs_0_), channel_id=1, source_target_pairs={{0,16},{8,24},{16,32},{24,40},{32,48},{40,56},{48,64},{56,72},{64,... | collective-permute-start | bytes 245768 | tf_op jit(solution)/shard_map/ppermute | solution.py:409
  113.0 9.0 %collective-permute-start.6 = (bf16[128,320]{1,0:T(8,128)(2,1)S(1)}, bf16[128,320]{1,0:T(8,128)(2,1)S(1)}, u32[]{:S(2)}, u32[]{:S(2)}) collective-permute-start(bf16[128,320]{1,0:T(8,128)(2,1)S(1)} %get-tuple-element.51.refs_2_), channel_id=1, source_target_pairs={{0,240},{8,248},{16,0},{24,8},{32,16},{40,24},{48,32},{56,40},{64,... | collective-permute-start | bytes 245768 | tf_op jit(solution)/shard_map/ppermute | solution.py:410
  122.0 18.9 %collective-permute-start.7 = (bf16[256,320]{1,0:T(8,128)(2,1)S(1)}, bf16[256,320]{1,0:T(8,128)(2,1)S(1)}, u32[]{:S(2)}, u32[]{:S(2)}) collective-permute-start(bf16[256,320]{1,0:T(8,128)(2,1)S(1)} %get-tuple-element.52), channel_id=1, source_target_pairs={{0,8},{8,16},{16,24},{24,32},{32,40},{40,48},{48,56},{56,64},{64,7... | collective-permute-start | bytes 491528 | tf_op jit(solution)/shard_map/ppermute | solution.py:419
  124.5 16.5 %collective-permute-start.8 = (bf16[256,320]{1,0:T(8,128)(2,1)S(1)}, bf16[256,320]{1,0:T(8,128)(2,1)S(1)}, u32[]{:S(2)}, u32[]{:S(2)}) collective-permute-start(bf16[256,320]{1,0:T(8,128)(2,1)S(1)} %get-tuple-element.53), channel_id=1, source_target_pairs={{0,248},{8,0},{16,8},{24,16},{32,24},{40,32},{48,40},{56,48},{64,5... | collective-permute-start | bytes 491528 | tf_op jit(solution)/shard_map/ppermute | solution.py:420
  128.6 17.9 %collective-permute-start.13 = (bf16[512,320]{1,0:T(8,128)(2,1)S(1)}, bf16[512,320]{1,0:T(8,128)(2,1)S(1)}, u32[]{:S(2)}, u32[]{:S(2)}) collective-permute-start(bf16[512,320]{1,0:T(8,128)(2,1)S(1)} %get-tuple-element.54.refs_4_), channel_id=1, source_target_pairs={{0,4},{4,0},{1,5},{5,1},{2,6},{6,2},{3,7},{7,3},{8,12},{12,8},{9,1... | collective-permute-start | bytes 983048 | tf_op jit(solution)/shard_map/ppermute | solution.py:422
  141.0 9.0 %collective-permute-start.12 = (bf16[512,320]{1,0:T(8,128)(2,1)S(1)}, bf16[512,320]{1,0:T(8,128)(2,1)S(1)}, u32[]{:S(2)}, u32[]{:S(2)}) collective-permute-start(bf16[512,320]{1,0:T(8,128)(2,1)S(1)} %assemble.7.refs_4_), channel_id=1, source_target_pairs={{0,4},{4,0},{1,5},{5,1},{2,6},{6,2},{3,7},{7,3},{8,12},{12,8},{9,1... | collective-permute-start | bytes 983048 | tf_op jit(solution)/shard_map/ppermute | solution.py:427
  151.5 13.3 %collective-permute-start.16 = (bf16[528,256]{1,0:T(8,128)(2,1)S(1)}, bf16[528,256]{1,0:T(8,128)(2,1)S(1)}, u32[]{:S(2)}, u32[]{:S(2)}) collective-permute-start(bf16[528,256]{1,0:T(8,128)(2,1)S(1)} %attend.13), channel_id=1, source_target_pairs={{0,1},{1,2},{2,3},{3,0},{4,5},{5,6},{6,7},{7,4},{8,9},{9,10},{10,1... | collective-permute-start | bytes 811016 | tf_op jit(solution)/shard_map/ppermute | solution.py:433
  155.3 9.5 %collective-permute-start.15 = (bf16[528,256]{1,0:T(8,128)(2,1)S(1)}, bf16[528,256]{1,0:T(8,128)(2,1)S(1)}, u32[]{:S(2)}, u32[]{:S(2)}) collective-permute-start(bf16[528,256]{1,0:T(8,128)(2,1)S(1)} %attend.12), channel_id=1, source_target_pairs={{0,3},{1,0},{2,1},{3,2},{4,7},{5,4},{6,5},{7,6},{8,11},{9,8},{10,9... | collective-permute-start | bytes 811016 | tf_op jit(solution)/shard_map/ppermute | solution.py:433
  161.2 10.6 %copy-start.1 = (bf16[256,512]{1,0:T(8,128)(2,1)S(1)}, bf16[256,512]{1,0:T(8,128)(2,1)}, u32[]{:S(2)}) copy-start(bf16[256,512]{1,0:T(8,128)(2,1)} %refs_3_.1) | copy-start | bytes 786436
  161.2 10.6 %copy-start.4 = (f32[512]{0:T(512)S(1)}, f32[512]{0:T(512)}, u32[]{:S(2)}) copy-start(f32[512]{0:T(512)} %param.18) | copy-start | bytes 6148
  161.2 10.5 %collective-permute-start.14 = (bf16[528,256]{1,0:T(8,128)(2,1)S(1)}, bf16[528,256]{1,0:T(8,128)(2,1)S(1)}, u32[]{:S(2)}, u32[]{:S(2)}) collective-permute-start(bf16[528,256]{1,0:T(8,128)(2,1)S(1)} %attend.11), channel_id=1, source_target_pairs={{0,2},{1,3},{2,0},{3,1},{4,6},{5,7},{6,4},{7,5},{8,10},{9,11},{10,... | collective-permute-start | bytes 811016 | tf_op jit(solution)/shard_map/ppermute | solution.py:433
  (1 other events, 1.0 us)
Sparse Core Ops, SparseCore 0:
  9.5 167.8 all-gather.2
